TPU v7x, 128 devices: a whole 4x4x4 slice. The times are simulated.
128 devices in a mesh: sp: 32 (over z, y, core), tp: 4 (over x).
Axes of the slice: x: 4, y: 4, z: 4, core: 2. Of those that a mesh axis runs over, the one named last changes fastest.
Arguments:
- resid: bfloat16 [16384, 2048], P(('sp', 'tp')), may hold values from -6 to 6
- query: bfloat16 [16384, 2048], P('sp', 'tp'), may hold values from -6 to 6
- forget_logits: bfloat16 [16384, 2048], P('sp', 'tp'), may hold values from -5 to 5
- forget_margin: float32 [2048], P('tp'), may hold values from 0 to 0.07, as said below
- decay_spike: float32 [16384, 16], P('sp', 'tp'), may hold values from -0.75 to 0
- value_logits: bfloat16 [16384, 2048], P('sp', 'tp'), may hold values from -6 to 6
- output_gate_logits: bfloat16 [16384, 2048], P('sp', 'tp'), may hold values from -6 to 6
- head_norm_scale: float32 [2048], P('tp'), may hold values from 0.1 to 1.9
- output_matrix: bfloat16 [2048, 2048], replicated, may hold values from -0.125 to 0.125
- norm_scale_vector: float32 [2048], replicated, may hold values from 0.1 to 1.9
- routes: int32 [16384, 2], P(('sp', 'tp')), may hold values from 0 to 127, all different within a row; in each aligned block of 128 rows (0 to 127, 128 to 255, ...) at most 4 rows name the same one
- routing_weight: float32 [16384, 2], P(('sp', 'tp')), may hold values from 0.2 to 1
- gate_matrix: bfloat16 [128, 2048, 1024], P(('sp', 'tp')), may hold values from -0.125 to 0.125
- up_matrix: bfloat16 [128, 2048, 1024], P(('sp', 'tp')), may hold values from -0.125 to 0.125
- down_matrix: bfloat16 [128, 1024, 2048], P(('sp', 'tp')), may hold values from -0.1875 to 0.1875
Outputs:
- result: bfloat16 [16384, 2048], P(('sp', 'tp'))
Inputs may be any that keep to these rules, and one draw needn't show every extreme that they name: `routes`: within the rows of one device no expert is named by more than 4 rows; some device names some expert exactly 4 times in every draw. `forget_margin`: Positive.
All inputs are finite; a program needn't handle non-finite values.
Results may differ from a plain program's by a relative error of at most 0.012.
Values may be sent and summed in bfloat16 or wider, within the bound.
No kernel may reach another device: no remote copies, remote signals or barrier semaphores. Data moves between devices by JAX's collectives and lax.ppermute only.
A program may use at most 128 MiB of HBM per device.

v0:
```python
import jax
import jax.numpy as jnp
from jax import lax
from jax.sharding import Mesh
from jax.sharding import PartitionSpec as P

DK = 128
BLOCK = 64
SP = ("sp_0", "sp_1", "sp_2")
SP_TP = ("sp_0", "sp_1", "sp_2", "tp")


maximum_value = lax.Precision.HIGHEST


def filled_with(value, identity):
    return jax.tree.map(
        lambda a, e: jnp.broadcast_to(jnp.asarray(e, a.dtype), a.shape), value, identity
    )


def carried_in(value, axes, combine, identity):
    before = start = filled_with(value, identity)
    so_far = value
    for axis in reversed(axes):
        devices, place = (lax.axis_size(axis), lax.axis_index(axis))
        pieces = jax.tree.map(lambda part: lax.all_gather(part, axis), so_far)
        inside, so_far = (start, start)
        for k in range(devices):
            passed = k < place
            so_far = combine(so_far, jax.tree.map(lambda part: part[k], pieces))
            inside = jax.tree.map(lambda new, old: jnp.where(passed, new, old), so_far, inside)
        before = combine(inside, before)
    return before


def in_blocks(value, dim, devices):
    lengths = value.shape
    parts = value.reshape(*lengths[:dim], devices, lengths[dim] // devices, *lengths[dim + 1 :])
    return jnp.moveaxis(parts, dim, 0)


def laid_out(parts, dim):
    parts = jnp.moveaxis(parts, 0, dim)
    lengths = parts.shape
    return parts.reshape(*lengths[:dim], lengths[dim] * lengths[dim + 1], *lengths[dim + 2 :])


def one_exchange(value, axis, axes, splits, concats):
    sizes = [lax.axis_size(a) for a in axes]
    parts = in_blocks(value, splits[0], sizes[0])
    parts = jnp.moveaxis(in_blocks(parts, splits[1] + 1, sizes[1]), 0, 1)
    inside = parts.shape[2:]
    parts = parts.reshape(-1, *inside)
    parts = lax.all_to_all(parts, axis, split_axis=0, concat_axis=0, tiled=True)
    parts = laid_out(parts.reshape(*sizes, *inside), concats[0] + 1)
    return laid_out(parts, concats[1])


def to_blocks(matrix, head_number):
    length, columns = matrix.shape
    return matrix.reshape(length // BLOCK, BLOCK, head_number, columns // head_number).transpose(
        0, 2, 1, 3
    )


def from_blocks(matrix):
    block_count, head_number, span_len, head_width = matrix.shape
    return matrix.transpose(0, 2, 1, 3).reshape(block_count * span_len, head_number * head_width)


def input_lookup(query, forget_logits, forget_margin, decay_spike, value_logits):
    head_number = decay_spike.shape[1]
    every_key = forget_margin[None, :] * jax.nn.sigmoid(-forget_logits.astype(jnp.float32))
    head_width = every_key.shape[1] // head_number
    logarithm_of_decay = jnp.log1p(-every_key) + jnp.repeat(decay_spike, head_width, axis=1)
    queries = query.astype(jnp.float32) * DK ** (-0.5)
    values = jax.nn.silu(value_logits.astype(jnp.float32))
    return (
        to_blocks(queries, head_number),
        to_blocks(every_key, head_number),
        to_blocks(values, head_number),
        to_blocks(logarithm_of_decay, head_number),
    )


def block_recurrence(queries, keys_in, values, logarithm_of_decay):
    span_len = queries.shape[2]
    causal = (
        lax.broadcasted_iota(jnp.int32, (span_len, span_len), 0)
        >= lax.broadcasted_iota(jnp.int32, (span_len, span_len), 1)
    )[:, :, None]
    cum_log = jnp.cumsum(logarithm_of_decay, axis=2)

    def advance(current_state, inputs):
        query_block, key_b, value_block, cumulative_block = inputs
        spread = cumulative_block[:, :, None, :] - cumulative_block[:, None, :, :]
        weight_t = jnp.where(causal, jnp.exp(jnp.where(causal, spread, 0.0)), 0.0)
        router_scores = jnp.einsum(
            "htk,hsk,htsk->hts", query_block, key_b, weight_t, precision=maximum_value
        )
        within = jnp.einsum("hts,hsv->htv", router_scores, value_block, precision=maximum_value)
        incoming_state = jnp.einsum(
            "bup,bpl->bul",
            query_block * jnp.exp(cumulative_block),
            current_state,
            precision=maximum_value,
        )
        final_block = cumulative_block[:, -1, :]
        decayed_state = key_b * jnp.exp(final_block[:, None, :] - cumulative_block)
        following_state = jnp.exp(final_block)[:, :, None] * current_state + jnp.einsum(
            "ixq,ixn->iqn", decayed_state, value_block, precision=maximum_value
        )
        return (following_state, within + incoming_state)

    start_state = jnp.zeros((queries.shape[1], queries.shape[3], values.shape[3]), jnp.float32)
    last_state, outputs = lax.scan(advance, start_state, (queries, keys_in, values, cum_log))
    return (last_state, outputs, cum_log)


def gate_rows(recurrence_output, output_gate_logits, head_norm_scale):
    square = jnp.mean(recurrence_output * recurrence_output, axis=3, keepdims=True)
    scaled = from_blocks(recurrence_output * lax.rsqrt(square + 1e-06)) * head_norm_scale[None, :]
    return (scaled * jax.nn.silu(output_gate_logits.astype(jnp.float32))).astype(jnp.bfloat16)


def row_norm(stream, norm_scale_vector):
    values = stream.astype(jnp.float32)
    square = jnp.mean(values * values, axis=1, keepdims=True)
    return (values * lax.rsqrt(square + 1e-06) * norm_scale_vector[None, :]).astype(jnp.bfloat16)


def join_states(earlier, later):
    early_log, early_state = earlier
    late_log, late_state = later
    return (early_log + late_log, jnp.exp(late_log)[:, :, None] * early_state + late_state)


def expert_block(slot_rows, gate_matrix, up_matrix, down_matrix):
    gate_part = jnp.einsum(
        "...ecd,edf->...ecf", slot_rows, gate_matrix, preferred_element_type=jnp.float32
    )
    up_part = jnp.einsum(
        "...ecd,edf->...ecf", slot_rows, up_matrix, preferred_element_type=jnp.float32
    )
    hidden = (jax.nn.silu(gate_part) * up_part).astype(jnp.bfloat16)
    return jnp.einsum(
        "...ecf,efd->...ecd", hidden, down_matrix, preferred_element_type=jnp.float32
    ).astype(jnp.bfloat16)


def body(
    resid,
    query,
    forget_logits,
    forget_margin,
    decay_spike,
    value_logits,
    output_gate_logits,
    head_norm_scale,
    output_matrix,
    norm_scale_vector,
    routes,
    routing_weight,
    gate_matrix,
    up_matrix,
    down_matrix,
):
    queries, keys_b, values, logarithm_of_decay = input_lookup(
        query, forget_logits, forget_margin, decay_spike, value_logits
    )
    last_state, recurrence_output, cum_log = block_recurrence(
        queries, keys_b, values, logarithm_of_decay
    )
    totals = cum_log[:, :, -1, :]
    before = jnp.cumsum(totals, axis=0) - totals
    device_log = jnp.sum(totals, axis=0)
    identity = (jnp.zeros_like(device_log), jnp.zeros_like(last_state))
    prior_state = carried_in((device_log, last_state), SP, join_states, identity)[1]
    readout_result = queries * jnp.exp(cum_log + before[:, :, None, :])
    recurrence_output = recurrence_output + jnp.einsum(
        "gwme,wej->gwmj", readout_result, prior_state, precision=maximum_value
    )
    gated_rows = gate_rows(recurrence_output, output_gate_logits, head_norm_scale)
    arrived_rows = lax.all_to_all(gated_rows, "tp", split_axis=0, concat_axis=1, tiled=True)
    mixed_rows = jnp.dot(arrived_rows, output_matrix, preferred_element_type=jnp.float32)
    stream = (resid.astype(jnp.float32) + mixed_rows).astype(jnp.bfloat16)
    normed = row_norm(stream, norm_scale_vector)
    row_count = routes.shape[0]
    top_count = routes.shape[1]
    model_width = normed.shape[1]
    per_device = gate_matrix.shape[0]
    devices = lax.axis_size(SP) * lax.axis_size("tp")
    experts = per_device * devices
    capacity = 2 * row_count * top_count // experts
    flat_routes = routes.reshape(-1)
    member = (flat_routes[:, None] == jnp.arange(experts, dtype=jnp.int32)[None, :]).astype(
        jnp.int32
    )
    slot_rank = jnp.sum(jnp.cumsum(member, axis=0) * member, axis=1) - 1
    position_entries = flat_routes * capacity + slot_rank
    select = (
        position_entries[:, None] == jnp.arange(experts * capacity, dtype=jnp.int32)[None, :]
    ).astype(jnp.bfloat16)
    select = select.reshape(row_count, top_count, experts * capacity)
    dispatch = jnp.sum(select, axis=1)
    packed = lax.dot_general(
        dispatch, normed, (((0,), (0,)), ((), ())), preferred_element_type=jnp.float32
    ).astype(jnp.bfloat16)
    sectioned = packed.reshape(
        lax.axis_size(SP), lax.axis_size("tp"), per_device, capacity, model_width
    )
    arrived = one_exchange(sectioned, SP_TP, (SP, "tp"), (0, 1), (0, 1))
    answers = expert_block(arrived, gate_matrix, up_matrix, down_matrix)
    returned = one_exchange(answers, SP_TP, (SP, "tp"), (0, 1), (0, 1))
    returned_rows = returned.reshape(experts * capacity, model_width)
    combined = stream.astype(jnp.float32)
    for pick_index in range(top_count):
        picked = jnp.dot(
            select[:, pick_index, :], returned_rows, preferred_element_type=jnp.float32
        )
        combined = combined + routing_weight[:, pick_index : pick_index + 1] * picked
    return combined.astype(jnp.bfloat16)


def solution(mesh):
    finer = Mesh(mesh.devices.reshape(4, 4, 2, mesh.shape["tp"]), ("sp_0", "sp_1", "sp_2", "tp"))
    placed = (
        P(SP_TP, None),
        P(SP, "tp"),
        P(SP, "tp"),
        P("tp"),
        P(SP, "tp"),
        P(SP, "tp"),
        P(SP, "tp"),
        P("tp"),
        P(),
        P(),
        P(SP_TP, None),
        P(SP_TP, None),
        P(SP_TP, None, None),
        P(SP_TP, None, None),
        P(SP_TP, None, None),
    )
    return jax.shard_map(
        body, mesh=finer, in_specs=placed, out_specs=P(SP_TP, None), check_vma=False
    )
```

profile of v0, /device:TPU:1, one launch (start us, length us, event | category | flops | bytes accessed | tf_op | source)
XLA Modules:
  0.0 324.6 jit_solution(18199731818932901205)
XLA Ops:
  8.0 2.6 divide_multiply_fusion
  20.2 113.1 %while.14 = (s32[]{:T(128)}, f32[4,128,128]{2,1,0:T(8,128)S(1)}, f32[8,4,64,128]{3,2,0,1:T(8,128)}, f32[8,4,64,128]{3,0,1,2:T(8,128)S(1)}, f32[8,4,64,128]{3,1,2...) while((s32[]{:T(128)}, f32[4,128,128]{2,1,0:T(8,128)S(1)}, ...), condition=%wide.region_2.3_spmd.clone.clone, body=%wide.region_1.2_spmd.clone.clone.sunk | while | flops 138792960 | bytes 20862588 | solution.py:117
  23.9 7.3 %fusion.164 = f32[4,64,64]{1,2,0:T(8,128)S(1)} fusion(f32[4,64,64,128]{3,2,1,0:T(8,128)S(1)} %exponential_select_fusion.2, f32[4,128,64]{1,2,0:T(8,128)S(1)} %dynamic-slice_bitcast_fusion.2, f32[4,128,64]{1,2,0:T(8,128)S(1)} %bitcast.352), kind=kLoop, calls=%fused_computation.2.clone.1 | loop fusion | flops 6275072 | bytes 8716288 | tf_op jit(solution)/shard_map/while/body/eval_jaxpr/htk,hsk,htsk->hts/dot_general | solution.py:99
  38.1 7.3 %fusion.164 = f32[4,64,64]{1,2,0:T(8,128)S(1)} fusion(f32[4,64,64,128]{3,2,1,0:T(8,128)S(1)} %exponential_select_fusion.2, f32[4,128,64]{1,2,0:T(8,128)S(1)} %dynamic-slice_bitcast_fusion.2, f32[4,128,64]{1,2,0:T(8,128)S(1)} %bitcast.352), kind=kLoop, calls=%fused_computation.2.clone.1 | loop fusion | flops 6275072 | bytes 8716288 | tf_op jit(solution)/shard_map/while/body/eval_jaxpr/htk,hsk,htsk->hts/dot_general | solution.py:99
  52.2 7.3 %fusion.164 = f32[4,64,64]{1,2,0:T(8,128)S(1)} fusion(f32[4,64,64,128]{3,2,1,0:T(8,128)S(1)} %exponential_select_fusion.2, f32[4,128,64]{1,2,0:T(8,128)S(1)} %dynamic-slice_bitcast_fusion.2, f32[4,128,64]{1,2,0:T(8,128)S(1)} %bitcast.352), kind=kLoop, calls=%fused_computation.2.clone.1 | loop fusion | flops 6275072 | bytes 8716288 | tf_op jit(solution)/shard_map/while/body/eval_jaxpr/htk,hsk,htsk->hts/dot_general | solution.py:99
  59.9 1.9 fusion.166
  66.4 7.3 %fusion.164 = f32[4,64,64]{1,2,0:T(8,128)S(1)} fusion(f32[4,64,64,128]{3,2,1,0:T(8,128)S(1)} %exponential_select_fusion.2, f32[4,128,64]{1,2,0:T(8,128)S(1)} %dynamic-slice_bitcast_fusion.2, f32[4,128,64]{1,2,0:T(8,128)S(1)} %bitcast.352), kind=kLoop, calls=%fused_computation.2.clone.1 | loop fusion | flops 6275072 | bytes 8716288 | tf_op jit(solution)/shard_map/while/body/eval_jaxpr/htk,hsk,htsk->hts/dot_general | solution.py:99
  74.1 1.9 fusion.166
  80.5 7.3 %fusion.164 = f32[4,64,64]{1,2,0:T(8,128)S(1)} fusion(f32[4,64,64,128]{3,2,1,0:T(8,128)S(1)} %exponential_select_fusion.2, f32[4,128,64]{1,2,0:T(8,128)S(1)} %dynamic-slice_bitcast_fusion.2, f32[4,128,64]{1,2,0:T(8,128)S(1)} %bitcast.352), kind=kLoop, calls=%fused_computation.2.clone.1 | loop fusion | flops 6275072 | bytes 8716288 | tf_op jit(solution)/shard_map/while/body/eval_jaxpr/htk,hsk,htsk->hts/dot_general | solution.py:99
  94.6 7.3 %fusion.164 = f32[4,64,64]{1,2,0:T(8,128)S(1)} fusion(f32[4,64,64,128]{3,2,1,0:T(8,128)S(1)} %exponential_select_fusion.2, f32[4,128,64]{1,2,0:T(8,128)S(1)} %dynamic-slice_bitcast_fusion.2, f32[4,128,64]{1,2,0:T(8,128)S(1)} %bitcast.352), kind=kLoop, calls=%fused_computation.2.clone.1 | loop fusion | flops 6275072 | bytes 8716288 | tf_op jit(solution)/shard_map/while/body/eval_jaxpr/htk,hsk,htsk->hts/dot_general | solution.py:99
  102.4 1.9 fusion.166
  108.8 7.3 %fusion.164 = f32[4,64,64]{1,2,0:T(8,128)S(1)} fusion(f32[4,64,64,128]{3,2,1,0:T(8,128)S(1)} %exponential_select_fusion.2, f32[4,128,64]{1,2,0:T(8,128)S(1)} %dynamic-slice_bitcast_fusion.2, f32[4,128,64]{1,2,0:T(8,128)S(1)} %bitcast.352), kind=kLoop, calls=%fused_computation.2.clone.1 | loop fusion | flops 6275072 | bytes 8716288 | tf_op jit(solution)/shard_map/while/body/eval_jaxpr/htk,hsk,htsk->hts/dot_general | solution.py:99
  116.5 1.9 fusion.166
  122.9 7.3 %fusion.164 = f32[4,64,64]{1,2,0:T(8,128)S(1)} fusion(f32[4,64,64,128]{3,2,1,0:T(8,128)S(1)} %exponential_select_fusion.2, f32[4,128,64]{1,2,0:T(8,128)S(1)} %dynamic-slice_bitcast_fusion.2, f32[4,128,64]{1,2,0:T(8,128)S(1)} %bitcast.352), kind=kLoop, calls=%fused_computation.2.clone.1 | loop fusion | flops 6275072 | bytes 8716288 | tf_op jit(solution)/shard_map/while/body/eval_jaxpr/htk,hsk,htsk->hts/dot_general | solution.py:99
  133.3 3.2 all-gather.1
  139.4 8.8 %all-gather.4 = f32[4,4,128]{2,1,0:T(4,128)S(1)} all-gather(f32[1,4,128]{2,1,0:T(4,128)S(1)} %get-tuple-element.149), channel_id=4, replica_groups=mesh['sp_0'=4,'sp_1'=4,'sp_2'=2,'tp'=4] {'sp_1'}, dimensions={0}, use_global_device_ids=true | all-gather | bytes 10240 | tf_op jit(solution)/shard_map/all_gather | solution.py:27
  148.2 15.5 %all-gather.8.cloned.1.call-done = f32[4,4,128,128]{3,2,1,0:T(8,128)} async-done(((f32[1,4,128,128]{3,2,1,0:T(8,128)}), f32[4,4,128,128]{3,2,1,0:T(8,128)}) %all-gather.8.cloned.1.call-update) | async-done | bytes 1048592 | tf_op jit(solution)/shard_map/all_gather | solution.py:27
  163.7 2.2 multiply_add_fusion
  166.8 8.8 %all_gather.31 = f32[4,4,128]{2,1,0:T(4,128)S(1)} all-gather(f32[1,4,128]{2,1,0:T(4,128)S(1)} %get-tuple-element.157), channel_id=1, replica_groups=mesh['sp_0'=4,'sp_1'=4,'sp_2'=2,'tp'=4] {'sp_0'}, dimensions={0}, use_global_device_ids=true | all-gather | bytes 10240 | tf_op jit(solution)/shard_map/all_gather | solution.py:27
  177.4 13.3 %all-gather.10.cloned.1.call-done = f32[4,4,128,128]{3,2,1,0:T(8,128)} async-done(((f32[1,4,128,128]{3,2,1,0:T(8,128)}), f32[4,4,128,128]{3,2,1,0:T(8,128)}) %all-gather.10.cloned.1.call-update) | async-done | bytes 1048592 | tf_op jit(solution)/shard_map/all_gather | solution.py:27
  190.7 4.7 %multiply_reduce_fusion.1 = (f32[8,4,64]{2,0,1:T(8,128)S(1)}, f32[8,4,64,128]{3,2,0,1:T(8,128)S(1)}) fusion(f32[8,4,64,128]{3,2,0,1:T(8,128)} %get-tuple-element.51, f32[8,4,64,128]{3,0,1,2:T(8,128)} %bitcast_multiply_fusion.8, f32[4,4,128,128]{3,2,1,0:T(8,128)} %all-gather.10.cloned.1.call-done, f32[4,4,128,128]{3,2,1,0:T(8,128)} %all-gather.8.cloned.1.call-done, ...), kind=kOutput, calls=%fused_computation.84 | convolution fusion | flops 405469184 | bytes 5799946 | tf_op jit(solution)/shard_map/gwme,wej->gwmj/dot_general | solution.py:181
  197.9 4.0 %all-to-all-start = ((bf16[4,128,512]{1,2,0:T(8,128)(2,1)}), bf16[4,128,512]{1,2,0:T(8,128)(2,1)S(1)}, u32[]{:S(2)}, u32[]{:S(2)}) async-start(bf16[4,128,512]{1,2,0:T(8,128)(2,1)} %copy.103), calls=%async_computation | async-start | bytes 1048576 | tf_op jit(solution)/shard_map/all_to_all | solution.py:185
  202.2 6.6 %all-to-all-done = bf16[4,128,512]{1,2,0:T(8,128)(2,1)S(1)} async-done(((bf16[4,128,512]{1,2,0:T(8,128)(2,1)}), bf16[4,128,512]{1,2,0:T(8,128)(2,1)S(1)}, u32[]{:S(2)}, u32[]{:S(2)}) %all-to-all-start) | async-done | bytes 524320 | tf_op jit(solution)/shard_map/all_to_all | solution.py:185
  208.8 4.8 %multiply_reduce_fusion = (f32[128]{0:T(128)S(1)}, f32[128,2048]{1,0:T(8,128)S(1)}) fusion(bf16[128,2048]{0,1:T(8,128)(2,1)S(1)} %bitcast.359, bf16[2048,2048]{1,0:T(8,128)(2,1)} %param.25, bf16[128,2048]{1,0:T(8,128)(2,1)S(1)} %copy-done.5), kind=kOutput, calls=%fused_computation.82 | convolution fusion | flops 1075314560 | bytes 10486272 | tf_op jit(solution)/shard_map/dot_general | solution.py:186
  214.3 2.2 reshape_transpose_transpose_reshape_reshape_reshape.3
  216.6 40.9 %all_to_all.29 = bf16[128,1,1,1,4,2048]{5,4,3,2,1,0:T(4,128)(2,1)S(1)} all-to-all(bf16[128,1,1,1,4,2048]{5,4,3,2,1,0:T(4,128)(2,1)} %bitcast.355), channel_id=1, replica_groups=mesh['sp_0'=4,'sp_1'=4,'sp_2'=2,'tp'=4] {'sp_0','sp_1','sp_2','tp'}, dimensions={0} | all-to-all | bytes 4194304 | tf_op jit(solution)/shard_map/all_to_all | solution.py:55
  257.5 4.7 %fusion.20 = f32[32,4,4,1024]{3,0,2,1:T(8,128)} fusion(bf16[1,2048,1024]{2,1,0:T(8,128)(2,1)S(1)} %copy-done.10, bf16[32,4,1,1,1,4,2048]{6,5,1,0,4,3,2:T(4,128)(2,1)S(1)} %bitcast.363), kind=kOutput, calls=%fused_computation.33 | convolution fusion | flops 2147483648 | bytes 8388608 | tf_op jit(solution)/shard_map/...ecd,edf->...ecf/dot_general | solution.py:143
  262.2 10.6 %fusion.27 = bf16[32,4,1,4,2048]{4,0,3,1,2:T(8,128)(2,1)} fusion(bf16[1,1024,2048]{2,1,0:T(8,128)(2,1)} %param.31, f32[32,4,4,1024]{3,0,2,1:T(8,128)} %fusion.20, bf16[1,2048,1024]{2,1,0:T(8,128)(2,1)} %param.29, bf16[32,4,1,1,1,4,2048]{6,5,1,0,4,3,2:T(4,128)(2,1)S(1)} %bitcast.364), kind=kOutput, calls=%fused_computation.39 | convolution fusion | flops 4299161600 | bytes 14680064 | tf_op jit(solution)/shard_map/...ecf,efd->...ecd/dot_general | solution.py:147
  272.8 4.5 %copy.111 = bf16[32,4,1,4,2048]{4,3,1,0,2:T(4,128)(2,1)} copy(bf16[32,4,1,4,2048]{4,0,3,1,2:T(8,128)(2,1)} %fusion.27) | data formatting | bytes 4194304 | tf_op jit(solution)/shard_map/convert_element_type | solution.py:149
  277.3 3.9 %all-to-all-start.2 = ((bf16[128,1,1,1,4,2048]{5,4,3,2,1,0:T(4,128)(2,1)}), bf16[128,1,1,1,4,2048]{5,4,3,2,1,0:T(4,128)(2,1)S(1)}, u32[]{:S(2)}, u32[]{:S(2)}) async-start(bf16[128,1,1,1,4,2048]{5,4,3,2,1,0:T(4,128)(2,1)} %bitcast.354), calls=%async_computation.2 | async-start | bytes 4194304 | tf_op jit(solution)/shard_map/all_to_all | solution.py:55
  281.4 30.7 %all-to-all-done.2 = bf16[128,1,1,1,4,2048]{5,4,3,2,1,0:T(4,128)(2,1)S(1)} async-done(((bf16[128,1,1,1,4,2048]{5,4,3,2,1,0:T(4,128)(2,1)}), bf16[128,1,1,1,4,2048]{5,4,3,2,1,0:T(4,128)(2,1)S(1)}, u32[]{:S(2)}, u32[]{:S(2)}) %all-to-all-start.2) | async-done | bytes 2097184 | tf_op jit(solution)/shard_map/all_to_all | solution.py:55
  313.5 2.5 reshape_reshape.3
  (168 shorter events, 69.4 us)
Async XLA Ops:
  6.5 157.1 %all-gather.8.cloned.1.call-start = ((), (), s32[]{:S(2)}) async-start(), calls=%async_computation.3 | async-start | bytes 1310720 | tf_op jit(solution)/shard_map/all_gather | solution.py:27
  10.6 2.7 copy-start.1
  12.0 2.7 copy-start.2
  14.7 1.7 copy-start.3
  133.3 32.7 %copy-start.7 = (s32[128,2]{0,1:T(2,128)S(1)}, s32[128,2]{0,1:T(2,128)}, u32[]{:S(2)}) copy-start(s32[128,2]{0,1:T(2,128)} %param.27) | copy-start | bytes 3076
  139.3 51.4 %all-gather.10.cloned.1.call-start = ((), (), s32[]{:S(2)}) async-start(), calls=%async_computation.4 | async-start | bytes 1310720 | tf_op jit(solution)/shard_map/all_gather | solution.py:27
  195.4 1.1 copy-start.4
  195.5 1.1 copy-start.8
  196.5 12.3 %copy-start.5 = (bf16[128,2048]{1,0:T(8,128)(2,1)S(1)}, bf16[128,2048]{1,0:T(8,128)(2,1)}, u32[]{:S(2)}) copy-start(bf16[128,2048]{1,0:T(8,128)(2,1)} %param.17) | copy-start | bytes 1572868
  197.9 10.9 %all-to-all-start = ((bf16[4,128,512]{1,2,0:T(8,128)(2,1)}), bf16[4,128,512]{1,2,0:T(8,128)(2,1)S(1)}, u32[]{:S(2)}, u32[]{:S(2)}) async-start(bf16[4,128,512]{1,2,0:T(8,128)(2,1)} %copy.103), calls=%async_computation | async-start | bytes 1048576 | tf_op jit(solution)/shard_map/all_to_all | solution.py:185
  208.8 4.8 %copy-start.6 = (f32[2048]{0:T(1024)S(1)}, f32[2048]{0:T(1024)}, u32[]{:S(2)}) copy-start(f32[2048]{0:T(1024)} %param.26) | copy-start | bytes 24580
  216.6 40.9 %copy-start.10 = (bf16[1,2048,1024]{2,1,0:T(8,128)(2,1)S(1)}, bf16[1,2048,1024]{2,1,0:T(8,128)(2,1)}, u32[]{:S(2)}) copy-start(bf16[1,2048,1024]{2,1,0:T(8,128)(2,1)} %param.30) | copy-start | bytes 12582916
  277.3 3.9 %copy-start.9 = (f32[128,2]{0,1:T(2,128)S(1)}, f32[128,2]{0,1:T(2,128)}, u32[]{:S(2)}) copy-start(f32[128,2]{0,1:T(2,128)} %param.28) | copy-start | bytes 3076
  277.3 34.8 %all-to-all-start.2 = ((bf16[128,1,1,1,4,2048]{5,4,3,2,1,0:T(4,128)(2,1)}), bf16[128,1,1,1,4,2048]{5,4,3,2,1,0:T(4,128)(2,1)S(1)}, u32[]{:S(2)}, u32[]{:S(2)}) async-start(bf16[128,1,1,1,4,2048]{5,4,3,2,1,0:T(4,128)(2,1)} %bitcast.354), calls=%async_computation.2 | async-start | bytes 4194304 | tf_op jit(solution)/shard_map/all_to_all | solution.py:55
  312.1 1.3 copy-start
Sparse Core Ops, SparseCore 0:
  139.4 24.1 all-gather.7
  166.0 24.6 all-gather.9
where the time goes:
time: 326 us; the launch traced here: 325 us
  other arithmetic  83.9 us (26%)
  waiting for transfers between devices  66.1 us (20%)
  blocking collectives  63.6 us (20%)
  matrix products  51.1 us (16%)
  local copies, waits for them, and re-layouts  37.7 us (12%)
  between operations  13.7 us (4%)
  starting transfers between devices  7.93 us (2%)
    dot_general x8, other arithmetic, advance(): jnp.einsum('htk,hsk,htsk->hts', query_block, key_b, weight_t, precision=m...  58.6 us
    all_to_all x1, blocking collectives, one_exchange(): parts = lax.all_to_all(parts, axis, split_axis=0, concat_axis=0, tiled=True)  40.9 us
    all_to_all x1, waiting for transfers between devices, one_exchange(): parts = lax.all_to_all(parts, axis, split_axis=0, concat_axis=0, tiled=True)  30.7 us
    all_gather x2, waiting for transfers between devices, carried_in(): pieces = jax.tree.map(lambda part: lax.all_gather(part, axis), so_far)  28.8 us
    all_gather x4, blocking collectives, carried_in(): pieces = jax.tree.map(lambda part: lax.all_gather(part, axis), so_far)  22.7 us
    dot_general x8, matrix products, advance(): jnp.einsum('bup,bpl->bul', query_block * jnp.exp(cumulative_block), curre...  15.4 us
    select_n x8, other arithmetic, advance(): weight_t = jnp.where(causal, jnp.exp(jnp.where(causal, spread, 0.0)), 0.0)  13.6 us
    dot_general x1, matrix products, expert_block(): jnp.einsum('...ecf,efd->...ecd', hidden, down_matrix, preferred_element_t...  10.6 us
  transfers between devices with their start and end apart: 4, of which 4 were waited for; matrix products, arithmetic and copies ran while one was open for 1% of the time, Pallas kernels for 0%

commit v1 on v0

v1 whole, which is shorter than its diff:
```python
import functools

import jax
import jax.numpy as jnp
from jax import lax
from jax.experimental import pallas as pl
from jax.experimental.pallas import tpu as pltpu
from jax.sharding import Mesh
from jax.sharding import PartitionSpec as P

DK = 128
CHUNK = 128
SP = ("sp_0", "sp_1", "sp_2")
SP_TP = ("sp_0", "sp_1", "sp_2", "tp")
F32 = jnp.float32
BF16 = jnp.bfloat16


def dot_nn(a, b):
    return lax.dot_general(a, b, (((1,), (0,)), ((), ())), preferred_element_type=F32)


def dot_nt(a, b):
    return lax.dot_general(a, b, (((1,), (1,)), ((), ())), preferred_element_type=F32)


def dot_tn(a, b):
    return lax.dot_general(a, b, (((0,), (0,)), ((), ())), preferred_element_type=F32)


def lower_mask(n, strict):
    row = lax.broadcasted_iota(jnp.int32, (n, n), 0)
    col = lax.broadcasted_iota(jnp.int32, (n, n), 1)
    return row > col if strict else row >= col


def in_hbm(value):
    return pltpu.with_memory_space_constraint(value, pltpu.HBM)


def params(mebibytes):
    return pltpu.CompilerParams(vmem_limit_bytes=mebibytes * 1024 * 1024)


def halves(value):
    high = value.astype(BF16)
    return high, (value - high.astype(F32)).astype(BF16)


def state_kernel(forget_ref, value_ref, margin_ref, spike_ref, cum_ref, values_ref, start_ref, sent_ref, state, before):
    step = pl.program_id(0)
    heads = forget_ref.shape[1] // DK

    @pl.when(step == 0)
    def _():
        state[...] = jnp.zeros_like(state)
        before[...] = jnp.zeros_like(before)

    tri = lower_mask(CHUNK, False).astype(BF16)
    for c in range(forget_ref.shape[0] // CHUNK):
        rows = slice(c * CHUNK, (c + 1) * CHUNK)
        spikes = halves(spike_ref[:, rows])
        spikes = dot_nt(tri, spikes[0]) + dot_nt(tri, spikes[1])
        start_ref[c] = state[...]
        for h in range(heads):
            cols = slice(h * DK, (h + 1) * DK)
            keys = margin_ref[:, cols] / (1.0 + jnp.exp(forget_ref[rows, cols].astype(F32)))
            high, low = halves(jnp.log(1.0 - keys))
            cum = dot_nn(tri, high) + dot_nn(tri, low) + spikes[:, h : h + 1]
            cum_ref[rows, cols] = cum
            last = cum[CHUNK - 1 : CHUNK, :]
            logits = value_ref[rows, cols].astype(F32)
            values = (logits / (1.0 + jnp.exp(-logits))).astype(BF16)
            values_ref[rows, cols] = values
            kept = (keys * jnp.exp(last - cum)).astype(BF16)
            state[cols, :] = jnp.exp(last) * state[cols, :] + dot_tn(values, kept)
            before[:, cols] = before[:, cols] + last

    @pl.when(step == pl.num_programs(0) - 1)
    def _():
        share = DK // 8
        first = lax.broadcasted_iota(jnp.int32, (share, DK), 0) == 0
        for h in range(heads):
            total = before[:, h * DK : (h + 1) * DK]
            high = total.astype(BF16).astype(F32)
            tail = jnp.where(first, high, total - high).astype(BF16)
            for i in range(8):
                row = h * DK + i * share
                sent_ref[h * 8 + i, 0:share, :] = state[row : row + share, :].astype(BF16)
                sent_ref[h * 8 + i, share : 2 * share, :] = tail


STATE_STEPS = 2


def local_states(forget_logits, value_logits, margin, spike):
    rows, width = forget_logits.shape
    heads = width // DK
    size = rows // STATE_STEPS
    by_rows = lambda i: (i, 0)
    return pl.pallas_call(
        state_kernel,
        grid=(STATE_STEPS,),
        in_specs=[
            pl.BlockSpec((size, width), by_rows),
            pl.BlockSpec((size, width), by_rows),
            pl.BlockSpec((1, width), lambda i: (0, 0)),
            pl.BlockSpec((heads, size), lambda i: (0, i)),
        ],
        out_specs=[
            pl.BlockSpec((size, width), by_rows),
            pl.BlockSpec((size, width), by_rows),
            pl.BlockSpec((size // CHUNK, width, DK), lambda i: (i, 0, 0)),
            pl.BlockSpec((heads * 8, 2 * DK // 8, DK), lambda i: (0, 0, 0)),
        ],
        out_shape=[
            pltpu.HBM((rows, width), F32),
            pltpu.HBM((rows, width), BF16),
            pltpu.HBM((rows // CHUNK, width, DK), F32),
            pltpu.HBM((heads * 8, 2 * DK // 8, DK), BF16),
        ],
        scratch_shapes=[pltpu.VMEM((width, DK), F32), pltpu.VMEM((1, width), F32)],
        compiler_params=params(16),
        name="local_states",
    )(*map(in_hbm, (forget_logits, value_logits, margin, spike)))


def carry_kernel(parts_ref, prior_ref):
    share = prior_ref.shape[1]
    running = jnp.zeros(prior_ref.shape[1:], F32)
    for d in range(parts_ref.shape[0]):
        prior_ref[d] = running
        tail = parts_ref[d, share : 2 * share, :].astype(F32)
        total = tail[0:1, :] + tail[1:2, :]
        running = jnp.exp(total) * running + parts_ref[d, 0:share, :].astype(F32)


def carried_in(parts):
    return pl.pallas_call(
        carry_kernel,
        out_shape=jax.ShapeDtypeStruct((parts.shape[0], parts.shape[1] // 2, parts.shape[2]), F32),
        compiler_params=params(8),
        name="carried_in",
    )(parts)


def dot_split(queries, states):
    return dot_nt(queries[0], states[0]) + dot_nt(queries[0], states[1]) + dot_nt(queries[1], states[0])


def within_kernel(query_ref, forget_ref, margin_ref, cum_ref, values_ref, start_ref, gate_ref, scale_ref, out_ref, high_ref, low_ref, gates_ref, before):
    heads = query_ref.shape[1] // DK
    causal = lower_mask(CHUNK, False)

    @pl.when(pl.program_id(0) == 0)
    def _():
        before[...] = jnp.zeros_like(before)

    for h in range(heads):
        cols = slice(h * DK, (h + 1) * DK)
        cum = cum_ref[:, cols]
        spread = cum - cum[CHUNK // 2 - 1 : CHUNK // 2, :]
        keys = margin_ref[:, cols] / (1.0 + jnp.exp(forget_ref[:, cols].astype(F32)))
        queries = query_ref[:, cols].astype(F32) * (DK**-0.5)
        scores = dot_nt((queries * jnp.exp(spread)).astype(BF16), (keys * jnp.exp(-spread)).astype(BF16))
        scores = jnp.where(causal, scores, 0.0).astype(BF16)
        decayed = queries * jnp.exp(cum)
        earlier = dot_split(halves(decayed), halves(start_ref[0, cols, :]))
        out_ref[:, cols] = dot_nn(scores, values_ref[:, cols]) + earlier
        high_ref[:, cols], low_ref[:, cols] = halves(decayed * jnp.exp(before[:, cols]))
        before[:, cols] = before[:, cols] + cum[CHUNK - 1 : CHUNK, :]
        logits = gate_ref[:, cols].astype(F32)
        gates_ref[:, cols] = scale_ref[:, cols] * (logits / (1.0 + jnp.exp(-logits)))


def within_blocks(query, forget_logits, margin, cum, values, start, gate_logits, scale):
    rows, width = query.shape
    block = pl.BlockSpec((CHUNK, width), lambda i: (i, 0))
    row = pl.BlockSpec((1, width), lambda i: (0, 0))
    return pl.pallas_call(
        within_kernel,
        grid=(rows // CHUNK,),
        in_specs=[block, block, row, block, block, pl.BlockSpec((1, width, DK), lambda i: (i, 0, 0)), block, row],
        out_specs=[block, block, block, block],
        out_shape=[pltpu.HBM((rows, width), kind) for kind in (F32, BF16, BF16, F32)],
        scratch_shapes=[pltpu.VMEM((1, width), F32)],
        compiler_params=params(16),
        name="within_blocks",
    )(*map(in_hbm, (query, forget_logits, margin, cum, values, start, gate_logits, scale)))


def readout_kernel(place_ref, within_ref, high_ref, low_ref, prior_ref, gates_ref, *out_refs):
    step = pl.program_id(0)
    heads = within_ref.shape[1] // DK
    parts = []
    for h in range(heads):
        cols = slice(h * DK, (h + 1) * DK)
        carried = dot_split((high_ref[:, cols], low_ref[:, cols]), halves(prior_ref[cols, :]))
        recurrent = within_ref[:, cols] + carried
        square = jnp.mean(recurrent * recurrent, axis=1, keepdims=True)
        parts.append((recurrent * lax.rsqrt(square + 1e-06) * gates_ref[:, cols]).astype(BF16))
    for k, out_ref in enumerate(out_refs):

        @pl.when(step == k)
        def _():
            for h in range(heads):
                out_ref[:, h * DK : (h + 1) * DK] = parts[h]


def gated_rows(place, within, high, low, prior, gates):
    rows, width = within.shape
    steps = rows // CHUNK
    block = pl.BlockSpec((CHUNK, width), lambda i, place: ((place[0] + i) % steps, 0))
    return pl.pallas_call(
        readout_kernel,
        grid_spec=pltpu.PrefetchScalarGridSpec(
            num_scalar_prefetch=1,
            grid=(steps,),
            in_specs=[block, block, block, pl.BlockSpec((width, DK), lambda i, place: (0, 0)), block],
            out_specs=[pl.BlockSpec((CHUNK, width), lambda i, place: (0, 0))] * steps,
        ),
        out_shape=[jax.ShapeDtypeStruct((CHUNK, width), BF16)] * steps,
        compiler_params=params(16),
        name="gated_rows",
    )(place, in_hbm(within), in_hbm(high), in_hbm(low), prior, in_hbm(gates))


def slot_positions(routes, experts, capacity):
    rows = routes.shape[0]
    lanes = lax.broadcasted_iota(jnp.int32, (rows, experts), 1)
    first, second = (routes[:, 0:1], routes[:, 1:2])
    one, two = (lanes == first, lanes == second)
    named = (one.astype(F32) + two.astype(F32)).astype(BF16)
    earlier = dot_nn(lower_mask(rows, True).astype(BF16), named)
    ranks = [
        jnp.sum(jnp.where(hit, earlier, 0.0), axis=1, keepdims=True).astype(jnp.int32)
        for hit in (one, two)
    ]
    return [expert * (2 * capacity) + rank for expert, rank in zip((first, second), ranks)]


def own_kernel(place_ref, own_ref, matrix_ref, resid_ref, routes_ref, total_ref, select_ref, pick_ref, *, experts, capacity):
    total_ref[...] = resid_ref[...].astype(F32) + dot_nn(own_ref[...], matrix_ref[...])
    rows = routes_ref.shape[0]
    slots = 2 * experts * capacity
    places = slot_positions(routes_ref[...], experts, capacity)
    lanes = lax.broadcasted_iota(jnp.int32, (rows, slots), 1)
    down = lax.broadcasted_iota(jnp.int32, (slots, rows), 0)
    across = [
        jnp.transpose(jnp.broadcast_to(place.astype(F32), (rows, rows)))[0:1, :].astype(jnp.int32)
        for place in places
    ]
    for j in range(2):
        hit = (down == across[0] + j * capacity) | (down == across[1] + j * capacity)
        select_ref[:, j * rows : (j + 1) * rows] = jnp.where(hit, 1.0, 0.0).astype(BF16)
        for k in range(2):
            at = (2 * j + k) * rows
            pick_ref[at : at + rows, :] = jnp.where(lanes == places[k] + j * capacity, 1.0, 0.0).astype(BF16)


def project_own(place, own, matrix, resid, routes, experts, capacity):
    rows, inner = own.shape
    width = matrix.shape[1]
    slots = 2 * experts * capacity
    fixed = lambda i, place: (0, 0)
    return pl.pallas_call(
        functools.partial(own_kernel, experts=experts, capacity=capacity),
        grid_spec=pltpu.PrefetchScalarGridSpec(
            num_scalar_prefetch=1,
            grid=(1,),
            in_specs=[
                pl.BlockSpec((rows, inner), fixed),
                pl.BlockSpec((inner, width), lambda i, place: (place[0], 0)),
                pl.BlockSpec((rows, width), fixed),
                pl.BlockSpec(routes.shape, fixed),
            ],
            out_specs=[
                pl.BlockSpec((rows, width), fixed),
                pl.BlockSpec((slots, 2 * rows), fixed),
                pl.BlockSpec((4 * rows, slots), fixed),
            ],
        ),
        out_shape=[
            jax.ShapeDtypeStruct((rows, width), F32),
            jax.ShapeDtypeStruct((slots, 2 * rows), BF16),
            jax.ShapeDtypeStruct((4 * rows, slots), BF16),
        ],
        compiler_params=params(24),
        name="project_own",
    )(place, own, in_hbm(matrix), in_hbm(resid), routes)


def project_kernel(place_ref, first_ref, second_ref, third_ref, matrix_ref, own_ref, scale_ref, select_ref, stream_ref, packed_ref, total, stacked):
    step = pl.program_id(0)
    for k, part_ref in enumerate((first_ref, second_ref, third_ref)):

        @pl.when(step == k)
        def _():
            total[...] = (own_ref if k == 0 else total)[...] + dot_nn(part_ref[...], matrix_ref[...])

    @pl.when(step == 2)
    def _():
        stream = total[...].astype(BF16)
        stream_ref[...] = stream
        values = stream.astype(F32)
        square = jnp.mean(values * values, axis=1, keepdims=True)
        normed = (values * lax.rsqrt(square + 1e-06) * scale_ref[...]).astype(BF16)
        rows, width = normed.shape
        half = width // 2
        stacked[0:rows, :] = normed[:, :half]
        stacked[rows : 2 * rows, :] = normed[:, half:]

    wide = packed_ref.shape[1]
    for n in range(stacked.shape[1] // wide):

        @pl.when(step == n + 2)
        def _():
            packed_ref[...] = dot_nn(select_ref[...], stacked[:, n * wide : (n + 1) * wide]).astype(BF16)


def project(place, arrived, shifts, matrix, own_total, scale, select):
    rows, inner = arrived[0].shape
    width = matrix.shape[1]
    parts = matrix.shape[0] // inner
    slots = select.shape[0]
    split = 4
    fixed = lambda i, place: (0, 0)

    def source(i, place):
        shift = jnp.where(i == 0, shifts[0], jnp.where(i == 1, shifts[1], shifts[2]))
        return ((place[0] + parts - shift) % parts, 0)

    return pl.pallas_call(
        project_kernel,
        grid_spec=pltpu.PrefetchScalarGridSpec(
            num_scalar_prefetch=1,
            grid=(2 + split,),
            in_specs=[
                pl.BlockSpec((rows, inner), fixed),
                pl.BlockSpec((rows, inner), fixed),
                pl.BlockSpec((rows, inner), fixed),
                pl.BlockSpec((inner, width), source),
                pl.BlockSpec((rows, width), fixed),
                pl.BlockSpec((1, width), fixed),
                pl.BlockSpec(select.shape, fixed),
            ],
            out_specs=[
                pl.BlockSpec((rows, width), fixed),
                pl.BlockSpec((slots, width // 2 // split), lambda i, place: (0, jnp.maximum(i - 2, 0))),
            ],
            scratch_shapes=[pltpu.VMEM((rows, width), F32), pltpu.VMEM((2 * rows, width // 2), BF16)],
        ),
        out_shape=[
            pltpu.HBM((rows, width), BF16),
            jax.ShapeDtypeStruct((slots, width // 2), BF16),
        ],
        compiler_params=params(24),
        name="project",
    )(place, *arrived, in_hbm(matrix), own_total, in_hbm(scale), select)


def expert_kernel(slots_ref, gate_ref, up_ref, down_ref, out_ref, rows_in, hidden, gate_in, up_in, down_in, outs, sems):
    half = slots_ref.shape[1]
    split, wide = (gate_in.shape[0], gate_in.shape[2])
    cols = [slice(i * wide, (i + 1) * wide) for i in range(split)]
    gate_copies = [pltpu.make_async_copy(gate_ref.at[0, :, cols[i]], gate_in.at[i], sems.at[0, i]) for i in range(split)]
    up_copies = [pltpu.make_async_copy(up_ref.at[0, :, cols[i]], up_in.at[i], sems.at[1, i]) for i in range(split)]
    down_copies = [
        [
            pltpu.make_async_copy(
                down_ref.at[0, :, j * half + i * wide : j * half + (i + 1) * wide], down_in.at[i, j], sems.at[2 + j, i]
            )
            for j in range(2)
        ]
        for i in range(split)
    ]
    out_copies = [pltpu.make_async_copy(outs.at[i], out_ref.at[:, cols[i]], sems.at[4, i]) for i in range(split)]
    for i in range(split):
        gate_copies[i].start()
        up_copies[i].start()
    for i in range(split):
        down_copies[i][0].start()
        down_copies[i][1].start()

    group = 64
    upper = lax.broadcasted_iota(jnp.int32, (group // 16, 8, half), 1) < 4

    def untangle(i, carry):
        block = slots_ref[pl.ds(i * group, group), :].astype(F32).reshape(group // 16, 2, 8, half)
        one, two = (block[:, 0], block[:, 1])
        low = jnp.where(upper, one, pltpu.roll(two, 4, 1))
        high = jnp.where(upper, pltpu.roll(one, 4, 1), two)
        at = pl.ds(i * (group // 2), group // 2)
        rows_in[at, 0:half] = low.reshape(group // 2, half).astype(BF16)
        rows_in[at, half : 2 * half] = high.reshape(group // 2, half).astype(BF16)
        return carry

    lax.fori_loop(0, slots_ref.shape[0] // group, untangle, 0)

    rows = rows_in.shape[0] // 2
    for i in range(split):
        gate_copies[i].wait()
        up_copies[i].wait()
        for m in range(2):
            at = slice(m * rows, (m + 1) * rows)
            gates = dot_nn(rows_in[at, :], gate_in[i])
            ups = dot_nn(rows_in[at, :], up_in[i])
            hidden[at, cols[i]] = (gates / (1.0 + jnp.exp(-gates)) * ups).astype(BF16)

    top = lax.broadcasted_iota(jnp.int32, (rows // 8, 8, wide), 1) < 4
    for i in range(split):
        down_copies[i][0].wait()
        down_copies[i][1].wait()
        for m in range(2):
            at = slice(m * rows, (m + 1) * rows)
            low = dot_nn(hidden[at, :], down_in[i, 0]).reshape(-1, 8, wide)
            high = dot_nn(hidden[at, :], down_in[i, 1]).reshape(-1, 8, wide)
            one = jnp.where(top, low, pltpu.roll(high, 4, 1))
            two = jnp.where(top, pltpu.roll(low, 4, 1), high)
            both = jnp.stack([one, two], axis=1).reshape(2 * rows, wide).astype(BF16)
            outs[i, 2 * m * rows : 2 * (m + 1) * rows, :] = both
        out_copies[i].start()
    for i in range(split):
        out_copies[i].wait()


def experts_on(slots, gate_matrix, up_matrix, down_matrix):
    rows, half = slots.shape
    width, inner = gate_matrix.shape[1:]
    split = 4
    wide = inner // split
    there = pl.BlockSpec(memory_space=pl.ANY)
    return pl.pallas_call(
        expert_kernel,
        in_specs=[pl.BlockSpec((rows, half), lambda: (0, 0)), there, there, there],
        out_specs=there,
        out_shape=pltpu.HBM((rows, half), BF16),
        scratch_shapes=[
            pltpu.VMEM((rows // 2, width), BF16),
            pltpu.VMEM((rows // 2, inner), BF16),
            pltpu.VMEM((split, width, wide), BF16),
            pltpu.VMEM((split, width, wide), BF16),
            pltpu.VMEM((split, 2, inner, half // split), BF16),
            pltpu.VMEM((split, rows, half // split), BF16),
            pltpu.SemaphoreType.DMA((5, split)),
        ],
        compiler_params=params(40),
        name="experts_on",
    )(slots, in_hbm(gate_matrix), in_hbm(up_matrix), in_hbm(down_matrix))


def combine_kernel(returned_ref, pick_ref, stream_ref, weight_ref, out_ref):
    rows, width = out_ref.shape
    half = returned_ref.shape[1]
    weights = weight_ref[...]
    wide = 256
    for n in range(half // wide):
        picked = dot_nn(pick_ref[...], returned_ref[:, n * wide : (n + 1) * wide])
        for j in range(2):
            at = 2 * j * rows
            cols = slice(j * half + n * wide, j * half + (n + 1) * wide)
            added = weights[:, 0:1] * picked[at : at + rows] + weights[:, 1:2] * picked[at + rows : at + 2 * rows]
            out_ref[:, cols] = (stream_ref[:, cols].astype(F32) + added).astype(BF16)


def combine(returned, pick, stream, routing_weight):
    return pl.pallas_call(
        combine_kernel,
        out_shape=jax.ShapeDtypeStruct(stream.shape, BF16),
        compiler_params=params(24),
        name="combine",
    )(returned, pick, in_hbm(stream), routing_weight)


def body(
    resid,
    query,
    forget_logits,
    forget_margin,
    decay_spike,
    value_logits,
    output_gate_logits,
    head_norm_scale,
    output_matrix,
    norm_scale_vector,
    routes,
    routing_weight,
    gate_matrix,
    up_matrix,
    down_matrix,
):
    rows, top = routes.shape
    experts = lax.axis_size(SP) * lax.axis_size("tp")
    capacity = 2 * rows * top // experts
    width = resid.shape[1]
    margin = forget_margin[None, :]
    places = lax.axis_size("tp")
    place = lax.axis_index("tp").astype(jnp.int32)[None]
    cum, values, start, sent = local_states(forget_logits, value_logits, margin, decay_spike.T)
    parts = lax.all_to_all(sent, SP, split_axis=0, concat_axis=0, tiled=True)
    within, high, low, gates = within_blocks(
        query, forget_logits, margin, cum, values, start, output_gate_logits, head_norm_scale[None, :]
    )
    prior = lax.all_to_all(carried_in(parts), SP, split_axis=0, concat_axis=0, tiled=True)
    gated = gated_rows(place, within, high, low, prior.reshape(start.shape[1], DK), gates)
    shifts = (1, places - 1, 2)
    sent_on = {
        k: lax.ppermute(gated[k], "tp", [(i, (i + k) % places) for i in range(places)]) for k in (2, 1, places - 1)
    }
    own, select, pick = project_own(place, gated[0], output_matrix, resid, routes, experts, capacity)
    stream, packed = project(
        place, [sent_on[k] for k in shifts], shifts, output_matrix, own, norm_scale_vector[None, :], select
    )
    shape = (experts, 2 * capacity, width // 2)
    slots = lax.all_to_all(packed.reshape(shape), SP_TP, split_axis=0, concat_axis=0, tiled=True)
    answers = experts_on(slots.reshape(packed.shape), gate_matrix, up_matrix, down_matrix)
    returned = lax.all_to_all(answers.reshape(shape), SP_TP, split_axis=0, concat_axis=0, tiled=True)
    return combine(returned.reshape(packed.shape), pick, stream, routing_weight)


def solution(mesh):
    finer = Mesh(mesh.devices.reshape(4, 4, 2, mesh.shape["tp"]), SP_TP)
    placed = (
        P(SP_TP, None),
        P(SP, "tp"),
        P(SP, "tp"),
        P("tp"),
        P(SP, "tp"),
        P(SP, "tp"),
        P(SP, "tp"),
        P("tp"),
        P(),
        P(),
        P(SP_TP, None),
        P(SP_TP, None),
        P(SP_TP, None, None),
        P(SP_TP, None, None),
        P(SP_TP, None, None),
    )
    return jax.shard_map(
        body, mesh=finer, in_specs=placed, out_specs=P(SP_TP, None), check_vma=False
    )
```

time: 326 us -> 143 us (0.44)
  other arithmetic: 83.9 us -> 0 us
  matrix products: 51.1 us -> 0 us
  Pallas kernels: 0 us -> 38.8 us
  local copies, waits for them, and re-layouts: 37.7 us -> 0.24 us
  waiting for transfers between devices: 66.1 us -> 36.9 us
  between operations: 13.7 us -> 0.09 us
  blocking collectives: 63.6 us -> 54.6 us
  starting transfers between devices: 7.93 us -> 12 us
    dot_general x8 -> x0, other arithmetic: 58.6 us -> none  [advance(): jnp.einsum('htk,hsk,htsk->hts', query_block, key_b, weight_t, precision=m...]
    dot_general x31 -> x0, matrix products: 51.1 us -> none  [the longest x8 15.4 us: advance(): jnp.einsum('bup,bpl->bul', query_block * jnp.exp(cumulative_block), curre...]
    pallas_call x0 -> x8, Pallas kernels: none -> 38.8 us  [the longest x1 10.5 us: experts_on(): pl.pallas_call(expert_kernel, in_specs=[pl.BlockSpec((rows, half), lambda...]
    all_gather x2 -> x0, waiting for transfers between devices: 28.8 us -> none  [carried_in(): pieces = jax.tree.map(lambda part: lax.all_gather(part, axis), so_far)]
    all_gather x4 -> x0, blocking collectives: 22.7 us -> none  [carried_in(): pieces = jax.tree.map(lambda part: lax.all_gather(part, axis), so_far)]
    all_to_all x1 -> x2, blocking collectives: 40.9 us -> 54.6 us  [the longest x1 36.1 us: body(): lax.all_to_all(packed.reshape(shape), SP_TP, split_axis=0, concat_axis=0,...]
    select_n x8 -> x0, other arithmetic: 13.6 us -> none  [advance(): weight_t = jnp.where(causal, jnp.exp(jnp.where(causal, spread, 0.0)), 0.0)]
    dynamic_slice x32 -> x0, local copies, waits for them, and re-layouts: 9.02 us -> none  [block_recurrence(): lax.scan(advance, start_state, (queries, keys_in, values, cum_log))]
  transfers between devices with their start and end apart: 4 -> 5, of which waited for: 4 -> 3; matrix products, arithmetic and copies ran while one was open for 1% -> 0% of each run, Pallas kernels for 0% -> 6%
where the time goes in v1:
time: 143 us
  blocking collectives  54.6 us (38%)
  Pallas kernels  38.8 us (27%)
  waiting for transfers between devices  36.9 us (26%)
  starting transfers between devices  12 us (8%)
    all_to_all x1, blocking collectives, body(): lax.all_to_all(packed.reshape(shape), SP_TP, split_axis=0, concat_axis=0,...  36.1 us
    all_to_all x1, waiting for transfers between devices, body(): lax.all_to_all(answers.reshape(shape), SP_TP, split_axis=0, concat_axis=0...  30.8 us
    all_to_all x1, blocking collectives, body(): parts = lax.all_to_all(sent, SP, split_axis=0, concat_axis=0, tiled=True)  18.5 us
    pallas_call x1, Pallas kernels, experts_on(): pl.pallas_call(expert_kernel, in_specs=[pl.BlockSpec((rows, half), lambda...  10.5 us
    pallas_call x1, Pallas kernels, project(): pl.pallas_call(project_kernel, grid_spec=pltpu.PrefetchScalarGridSpec(num...  6.79 us
    pallas_call x1, Pallas kernels, within_blocks(): pl.pallas_call(within_kernel, grid=(rows // CHUNK,), in_specs=[block, blo...  5.55 us
    pallas_call x1, Pallas kernels, local_states(): pl.pallas_call(state_kernel, grid=(STATE_STEPS,), in_specs=[pl.BlockSpec(...  5.21 us
    ppermute x3, starting transfers between devices, body(): lax.ppermute(gated[k], 'tp', [(i, (i + k) % places) for i in range(places)])  4.28 us
  transfers between devices with their start and end apart: 5, of which 3 were waited for; matrix products, arithmetic and copies ran while one was open for 0% of the time, Pallas kernels for 6%

profile of v1, /device:TPU:1, one launch (start us, length us, event | category | flops | bytes accessed | tf_op | source)
XLA Modules:
  0.0 142.6 jit_solution(303754153757285815)
XLA Ops:
  0.0 5.2 %local_states.1 = (f32[512,512]{1,0:T(8,128)}, bf16[512,512]{1,0:T(8,128)(2,1)}, f32[4,512,128]{2,1,0:T(8,128)}, bf16[32,32,128]{2,1,0:T(8,128)(2,1)}) custom-call(bf16[512,512]{1,0:T(8,128)(2,1)} %forget_ref.3, bf16[512,512]{1,0:T(8,128)(2,1)} %value_ref.1, f32[1,512]{1,0:T(1,128)} %bitcast.15, f32[4,512]{1,0:T(4,128)} %bitcast.17), custom_call_target="tpu_custom_call" | custom-call | tf_op jit(solution)/shard_map/local_states/pallas_call | solution.py:101
  5.2 18.5 %all_to_all.20.parts_ref = bf16[32,32,128]{2,1,0:T(8,128)(2,1)S(1)} all-to-all(bf16[32,32,128]{2,1,0:T(8,128)(2,1)} %get-tuple-element.28), channel_id=1, replica_groups=mesh['sp_0'=4,'sp_1'=4,'sp_2'=2,'tp'=4] {'sp_0','sp_1','sp_2'}, dimensions={0} | all-to-all | bytes 524288 | tf_op jit(solution)/shard_map/all_to_all | solution.py:500
  23.7 0.8 carried_in.1
  24.5 0.0 copy-start
  24.5 3.9 %all-to-all-start.1 = ((f32[32,16,128]{2,1,0:T(8,128)}), f32[32,16,128]{2,1,0:T(8,128)S(1)}, u32[]{:S(2)}, u32[]{:S(2)}) async-start(f32[32,16,128]{2,1,0:T(8,128)} %carried_in.1), calls=%async_computation.1 | async-start | bytes 524288 | tf_op jit(solution)/shard_map/all_to_all | solution.py:504
  28.4 5.5 %within_blocks.1 = (f32[512,512]{1,0:T(8,128)}, bf16[512,512]{1,0:T(8,128)(2,1)}, bf16[512,512]{1,0:T(8,128)(2,1)}, f32[512,512]{1,0:T(8,128)}) custom-call(bf16[512,512]{1,0:T(8,128)(2,1)} %query_ref.1, bf16[512,512]{1,0:T(8,128)(2,1)} %forget_ref.3, f32[1,512]{1,0:T(1,128)} %bitcast.16, f32[512,512]{1,0:T(8,128)} %get-tuple-element.22.cum_ref, ...), custom_call_target="tpu_custom_call" | custom-call | tf_op jit(solution)/shard_map/within_blocks/pallas_call | solution.py:180
  33.9 3.3 %all-to-all-done.1 = f32[32,16,128]{2,1,0:T(8,128)S(1)} async-done(((f32[32,16,128]{2,1,0:T(8,128)}), f32[32,16,128]{2,1,0:T(8,128)S(1)}, u32[]{:S(2)}, u32[]{:S(2)}) %all-to-all-start.1) | async-done | bytes 262176 | tf_op jit(solution)/shard_map/all_to_all | solution.py:504
  37.3 4.1 %gated_rows.1 = (bf16[128,512]{1,0:T(8,128)(2,1)S(1)}, bf16[128,512]{1,0:T(8,128)(2,1)S(1)}, bf16[128,512]{1,0:T(8,128)(2,1)S(1)}, bf16[128,512]{1,0:T(8,128)(2,1)S(1)}) custom-call(s32[1]{0:T(128)} %bitcast.place_ref, f32[512,512]{1,0:T(8,128)} %get-tuple-element.25.within_ref, bf16[512,512]{1,0:T(8,128)(2,1)} %get-tuple-element.26.high_ref, ...), custom_call_target="tpu_custom_call" | custom-call | tf_op jit(solution)/shard_map/gated_rows/pallas_call | solution.py:214
  41.3 1.3 collective-permute-start
  42.6 1.5 %collective-permute-start.1 = (bf16[128,512]{1,0:T(8,128)(2,1)S(1)}, bf16[128,512]{1,0:T(8,128)(2,1)S(1)}, u32[]{:S(2)}, u32[]{:S(2)}) collective-permute-start(bf16[128,512]{1,0:T(8,128)(2,1)S(1)} %get-tuple-element.31), channel_id=1, source_target_pairs={{0,3},{1,0},{2,1},{3,2},{4,7},{5,4},{6,5},{7,6},{8,11},{9,8},{10,9... | collective-permute-start | bytes 393224 | tf_op jit(solution)/shard_map/ppermute | solution.py:508
  44.1 1.5 %collective-permute-start.2 = (bf16[128,512]{1,0:T(8,128)(2,1)S(1)}, bf16[128,512]{1,0:T(8,128)(2,1)S(1)}, u32[]{:S(2)}, u32[]{:S(2)}) collective-permute-start(bf16[128,512]{1,0:T(8,128)(2,1)S(1)} %get-tuple-element.32), channel_id=1, source_target_pairs={{0,2},{1,3},{2,0},{3,1},{4,6},{5,7},{6,4},{7,5},{8,10},{9,11},{10,... | collective-permute-start | bytes 393224 | tf_op jit(solution)/shard_map/ppermute | solution.py:508
  45.6 0.0 copy-done
  45.6 0.1 copy.16.routes_ref
  45.7 2.8 %project_own.1 = (f32[128,2048]{1,0:T(8,128)S(1)}, bf16[1024,256]{1,0:T(8,128)(2,1)S(1)}, bf16[512,1024]{1,0:T(8,128)(2,1)S(1)}) custom-call(s32[1]{0:T(128)} %bitcast.place_ref, bf16[128,512]{1,0:T(8,128)(2,1)S(1)} %get-tuple-element.33.own_ref, bf16[2048,2048]{1,0:T(8,128)(2,1)} %matrix_ref.3, bf16[128,2048]{1,0:T(8,128)(2,1)} %resid_ref.1, ...), custom_call_target="tpu_custom_call" | custom-call | tf_op jit(solution)/shard_map/project_own/pallas_call | solution.py:266
  48.5 0.0 collective-permute-done.first_ref
  48.5 0.0 collective-permute-done.1.second_ref
  48.5 2.8 %collective-permute-done.2.third_ref = bf16[128,512]{1,0:T(8,128)(2,1)S(1)} collective-permute-done((bf16[128,512]{1,0:T(8,128)(2,1)S(1)}, bf16[128,512]{1,0:T(8,128)(2,1)S(1)}, u32[]{:S(2)}, u32[]{:S(2)}) %collective-permute-start.2) | collective-permute-done | bytes 131104 | tf_op jit(solution)/shard_map/ppermute | solution.py:508
  51.3 6.8 %project.1 = (bf16[128,2048]{1,0:T(8,128)(2,1)}, bf16[1024,1024]{1,0:T(8,128)(2,1)S(1)}) custom-call(s32[1]{0:T(128)} %bitcast.place_ref, bf16[128,512]{1,0:T(8,128)(2,1)S(1)} %collective-permute-done.first_ref, bf16[128,512]{1,0:T(8,128)(2,1)S(1)} %collective-permute-done.1.second_ref, bf16[128,512]{1,0:T(8,128)(2,1)S(1)} %collective-permute-done.2.third_ref, ...), custom_call_target="tpu_custom_call" | custom-call | tf_op jit(solution)/shard_map/project/pallas_call | solution.py:333
  58.1 36.1 %all_to_all.21 = bf16[128,8,1024]{2,1,0:T(8,128)(2,1)S(1)} all-to-all(bf16[128,8,1024]{2,1,0:T(8,128)(2,1)S(1)} %bitcast.12), channel_id=1, replica_groups=mesh['sp_0'=4,'sp_1'=4,'sp_2'=2,'tp'=4] {'sp_0','sp_1','sp_2','tp'}, dimensions={0} | all-to-all | bytes 4194304 | tf_op jit(solution)/shard_map/all_to_all | solution.py:515
  94.2 10.5 %experts_on.1 = bf16[1024,1024]{1,0:T(8,128)(2,1)} custom-call(bf16[1024,1024]{1,0:T(8,128)(2,1)S(1)} %bitcast.11, bf16[1,2048,1024]{2,1,0:T(8,128)(2,1)} %gate_ref.3, bf16[1,2048,1024]{2,1,0:T(8,128)(2,1)} %up_ref.1, bf16[1,1024,2048]{2,1,0:T(8,128)(2,1)} %down_ref.1), custom_call_target="tpu_custom_call" | custom-call | tf_op jit(solution)/shard_map/experts_on/pallas_call | solution.py:433
  104.8 0.0 copy-start.1
  104.8 3.8 %all-to-all-start.3 = ((bf16[128,8,1024]{2,1,0:T(8,128)(2,1)}), bf16[128,8,1024]{2,1,0:T(8,128)(2,1)S(1)}, u32[]{:S(2)}, u32[]{:S(2)}) async-start(bf16[128,8,1024]{2,1,0:T(8,128)(2,1)} %bitcast.14), calls=%async_computation.3 | async-start | bytes 4194304 | tf_op jit(solution)/shard_map/all_to_all | solution.py:517
  108.6 0.0 copy-done.1
  108.6 0.1 copy.17.weight_ref
  108.7 30.8 %all-to-all-done.3 = bf16[128,8,1024]{2,1,0:T(8,128)(2,1)S(1)} async-done(((bf16[128,8,1024]{2,1,0:T(8,128)(2,1)}), bf16[128,8,1024]{2,1,0:T(8,128)(2,1)S(1)}, u32[]{:S(2)}, u32[]{:S(2)}) %all-to-all-start.3) | async-done | bytes 2097184 | tf_op jit(solution)/shard_map/all_to_all | solution.py:517
  139.5 3.1 %combine.1 = bf16[128,2048]{1,0:T(8,128)(2,1)} custom-call(bf16[1024,1024]{1,0:T(8,128)(2,1)S(1)} %bitcast.10, bf16[512,1024]{1,0:T(8,128)(2,1)S(1)} %get-tuple-element.37.pick_ref, bf16[128,2048]{1,0:T(8,128)(2,1)} %get-tuple-element.38.stream_ref, f32[128,2]{1,0:T(8,128)S(1)} %copy.17.weight_ref), custom_call_target="tpu_custom_call" | custom-call | tf_op jit(solution)/shard_map/combine/pallas_call | solution.py:467
Async XLA Ops:
  24.5 21.1 %copy-start = (s32[128,2]{0,1:T(2,128)S(1)}, s32[128,2]{0,1:T(2,128)}, u32[]{:S(2)}) copy-start(s32[128,2]{0,1:T(2,128)} %param.25) | copy-start | bytes 3076
  24.5 12.8 %all-to-all-start.1 = ((f32[32,16,128]{2,1,0:T(8,128)}), f32[32,16,128]{2,1,0:T(8,128)S(1)}, u32[]{:S(2)}, u32[]{:S(2)}) async-start(f32[32,16,128]{2,1,0:T(8,128)} %carried_in.1), calls=%async_computation.1 | async-start | bytes 524288 | tf_op jit(solution)/shard_map/all_to_all | solution.py:504
  41.3 7.2 %collective-permute-start = (bf16[128,512]{1,0:T(8,128)(2,1)S(1)}, bf16[128,512]{1,0:T(8,128)(2,1)S(1)}, u32[]{:S(2)}, u32[]{:S(2)}) collective-permute-start(bf16[128,512]{1,0:T(8,128)(2,1)S(1)} %get-tuple-element.30), channel_id=1, source_target_pairs={{0,1},{1,2},{2,3},{3,0},{4,5},{5,6},{6,7},{7,4},{8,9},{9,10},{10,1... | collective-permute-start | bytes 393224 | tf_op jit(solution)/shard_map/ppermute | solution.py:508
  42.6 5.9 %collective-permute-start.1 = (bf16[128,512]{1,0:T(8,128)(2,1)S(1)}, bf16[128,512]{1,0:T(8,128)(2,1)S(1)}, u32[]{:S(2)}, u32[]{:S(2)}) collective-permute-start(bf16[128,512]{1,0:T(8,128)(2,1)S(1)} %get-tuple-element.31), channel_id=1, source_target_pairs={{0,3},{1,0},{2,1},{3,2},{4,7},{5,4},{6,5},{7,6},{8,11},{9,8},{10,9... | collective-permute-start | bytes 393224 | tf_op jit(solution)/shard_map/ppermute | solution.py:508
  44.1 7.2 %collective-permute-start.2 = (bf16[128,512]{1,0:T(8,128)(2,1)S(1)}, bf16[128,512]{1,0:T(8,128)(2,1)S(1)}, u32[]{:S(2)}, u32[]{:S(2)}) collective-permute-start(bf16[128,512]{1,0:T(8,128)(2,1)S(1)} %get-tuple-element.32), channel_id=1, source_target_pairs={{0,2},{1,3},{2,0},{3,1},{4,6},{5,7},{6,4},{7,5},{8,10},{9,11},{10,... | collective-permute-start | bytes 393224 | tf_op jit(solution)/shard_map/ppermute | solution.py:508
  104.8 3.8 %copy-start.1 = (f32[128,2]{0,1:T(2,128)S(1)}, f32[128,2]{0,1:T(2,128)}, u32[]{:S(2)}) copy-start(f32[128,2]{0,1:T(2,128)} %param.26) | copy-start | bytes 3076
  104.8 34.7 %all-to-all-start.3 = ((bf16[128,8,1024]{2,1,0:T(8,128)(2,1)}), bf16[128,8,1024]{2,1,0:T(8,128)(2,1)S(1)}, u32[]{:S(2)}, u32[]{:S(2)}) async-start(bf16[128,8,1024]{2,1,0:T(8,128)(2,1)} %bitcast.14), calls=%async_computation.3 | async-start | bytes 4194304 | tf_op jit(solution)/shard_map/all_to_all | solution.py:517

commit v2 on v1

v2 whole, which is shorter than its diff:
```python
import functools

import jax
import jax.numpy as jnp
from jax import lax
from jax.experimental import pallas as pl
from jax.experimental.pallas import tpu as pltpu
from jax.sharding import Mesh
from jax.sharding import PartitionSpec as P

DK = 128
CHUNK = 128
SP = ("sp_0", "sp_1", "sp_2")
SP_TP = ("sp_0", "sp_1", "sp_2", "tp")
F32 = jnp.float32
BF16 = jnp.bfloat16


def dot_nn(a, b):
    return lax.dot_general(a, b, (((1,), (0,)), ((), ())), preferred_element_type=F32)


def dot_nt(a, b):
    return lax.dot_general(a, b, (((1,), (1,)), ((), ())), preferred_element_type=F32)


def dot_tn(a, b):
    return lax.dot_general(a, b, (((0,), (0,)), ((), ())), preferred_element_type=F32)


def lower_mask(n, strict):
    row = lax.broadcasted_iota(jnp.int32, (n, n), 0)
    col = lax.broadcasted_iota(jnp.int32, (n, n), 1)
    return row > col if strict else row >= col


def in_hbm(value):
    return pltpu.with_memory_space_constraint(value, pltpu.HBM)


def in_vmem(value):
    return pltpu.with_memory_space_constraint(value, pltpu.VMEM)


def params(mebibytes):
    return pltpu.CompilerParams(vmem_limit_bytes=mebibytes * 1024 * 1024)


def halves(value):
    high = value.astype(BF16)
    return high, (value - high.astype(F32)).astype(BF16)


def state_kernel(forget_ref, value_ref, margin_ref, spike_ref, cum_ref, values_ref, start_ref, sent_ref, state, before):
    step = pl.program_id(0)
    heads = forget_ref.shape[1] // DK

    @pl.when(step == 0)
    def _():
        state[...] = jnp.zeros_like(state)
        before[...] = jnp.zeros_like(before)

    tri = lower_mask(CHUNK, False).astype(BF16)
    for c in range(forget_ref.shape[0] // CHUNK):
        rows = slice(c * CHUNK, (c + 1) * CHUNK)
        spikes = halves(spike_ref[:, rows])
        spikes = dot_nt(tri, spikes[0]) + dot_nt(tri, spikes[1])
        start_ref[c] = state[...]
        for h in range(heads):
            cols = slice(h * DK, (h + 1) * DK)
            keys = margin_ref[:, cols] / (1.0 + jnp.exp(forget_ref[rows, cols].astype(F32)))
            high, low = halves(jnp.log(1.0 - keys))
            cum = dot_nn(tri, high) + dot_nn(tri, low) + spikes[:, h : h + 1]
            cum_ref[rows, cols] = cum
            last = cum[CHUNK - 1 : CHUNK, :]
            logits = value_ref[rows, cols].astype(F32)
            values = (logits / (1.0 + jnp.exp(-logits))).astype(BF16)
            values_ref[rows, cols] = values
            kept = (keys * jnp.exp(last - cum)).astype(BF16)
            state[cols, :] = jnp.exp(last) * state[cols, :] + dot_tn(values, kept)
            before[:, cols] = before[:, cols] + last

    @pl.when(step == pl.num_programs(0) - 1)
    def _():
        share = DK // 8
        first = lax.broadcasted_iota(jnp.int32, (share, DK), 0) == 0
        for h in range(heads):
            total = before[:, h * DK : (h + 1) * DK]
            high = total.astype(BF16).astype(F32)
            tail = jnp.where(first, high, total - high).astype(BF16)
            for i in range(8):
                row = h * DK + i * share
                sent_ref[h * 8 + i, 0:share, :] = state[row : row + share, :].astype(BF16)
                sent_ref[h * 8 + i, share : 2 * share, :] = tail


STATE_STEPS = 2


def local_states(forget_logits, value_logits, margin, spike):
    rows, width = forget_logits.shape
    heads = width // DK
    size = rows // STATE_STEPS
    by_rows = lambda i: (i, 0)
    return pl.pallas_call(
        state_kernel,
        grid=(STATE_STEPS,),
        in_specs=[
            pl.BlockSpec((size, width), by_rows),
            pl.BlockSpec((size, width), by_rows),
            pl.BlockSpec((1, width), lambda i: (0, 0)),
            pl.BlockSpec((heads, size), lambda i: (0, i)),
        ],
        out_specs=[
            pl.BlockSpec((size, width), by_rows),
            pl.BlockSpec((size, width), by_rows),
            pl.BlockSpec((size // CHUNK, width, DK), lambda i: (i, 0, 0)),
            pl.BlockSpec((heads * 8, 2 * DK // 8, DK), lambda i: (0, 0, 0)),
        ],
        out_shape=[
            pltpu.HBM((rows, width), F32),
            pltpu.HBM((rows, width), BF16),
            pltpu.HBM((rows // CHUNK, width, DK), F32),
            pltpu.HBM((heads * 8, 2 * DK // 8, DK), BF16),
        ],
        scratch_shapes=[pltpu.VMEM((width, DK), F32), pltpu.VMEM((1, width), F32)],
        compiler_params=params(16),
        name="local_states",
    )(*map(in_hbm, (forget_logits, value_logits, margin, spike)))


def carry_kernel(parts_ref, prior_ref):
    share = prior_ref.shape[1]
    running = jnp.zeros(prior_ref.shape[1:], F32)
    for d in range(parts_ref.shape[0]):
        prior_ref[d] = running
        tail = parts_ref[d, share : 2 * share, :].astype(F32)
        total = tail[0:1, :] + tail[1:2, :]
        running = jnp.exp(total) * running + parts_ref[d, 0:share, :].astype(F32)


def carried_in(parts):
    return pl.pallas_call(
        carry_kernel,
        out_shape=jax.ShapeDtypeStruct((parts.shape[0], parts.shape[1] // 2, parts.shape[2]), F32),
        compiler_params=params(8),
        name="carried_in",
    )(parts)


def dot_split(queries, states):
    return dot_nt(queries[0], states[0]) + dot_nt(queries[0], states[1]) + dot_nt(queries[1], states[0])


def within_kernel(query_ref, forget_ref, margin_ref, cum_ref, values_ref, start_ref, gate_ref, scale_ref, out_ref, high_ref, low_ref, gates_ref, before):
    heads = query_ref.shape[1] // DK
    causal = lower_mask(CHUNK, False)

    @pl.when(pl.program_id(0) == 0)
    def _():
        before[...] = jnp.zeros_like(before)

    for h in range(heads):
        cols = slice(h * DK, (h + 1) * DK)
        cum = cum_ref[:, cols]
        spread = cum - cum[CHUNK // 2 - 1 : CHUNK // 2, :]
        keys = margin_ref[:, cols] / (1.0 + jnp.exp(forget_ref[:, cols].astype(F32)))
        queries = query_ref[:, cols].astype(F32) * (DK**-0.5)
        scores = dot_nt((queries * jnp.exp(spread)).astype(BF16), (keys * jnp.exp(-spread)).astype(BF16))
        scores = jnp.where(causal, scores, 0.0).astype(BF16)
        decayed = queries * jnp.exp(cum)
        earlier = dot_split(halves(decayed), halves(start_ref[0, cols, :]))
        out_ref[:, cols] = dot_nn(scores, values_ref[:, cols]) + earlier
        high_ref[:, cols], low_ref[:, cols] = halves(decayed * jnp.exp(before[:, cols]))
        before[:, cols] = before[:, cols] + cum[CHUNK - 1 : CHUNK, :]
        logits = gate_ref[:, cols].astype(F32)
        gates_ref[:, cols] = scale_ref[:, cols] * (logits / (1.0 + jnp.exp(-logits)))


def within_blocks(query, forget_logits, margin, cum, values, start, gate_logits, scale):
    rows, width = query.shape
    block = pl.BlockSpec((CHUNK, width), lambda i: (i, 0))
    row = pl.BlockSpec((1, width), lambda i: (0, 0))
    return pl.pallas_call(
        within_kernel,
        grid=(rows // CHUNK,),
        in_specs=[block, block, row, block, block, pl.BlockSpec((1, width, DK), lambda i: (i, 0, 0)), block, row],
        out_specs=[block, block, block, block],
        out_shape=[pltpu.VMEM((rows, width), kind) for kind in (F32, BF16, BF16, F32)],
        scratch_shapes=[pltpu.VMEM((1, width), F32)],
        compiler_params=params(24),
        name="within_blocks",
    )(*map(in_hbm, (query, forget_logits, margin, cum, values, start, gate_logits, scale)))


def readout_kernel(within_ref, high_ref, low_ref, prior_ref, gates_ref, out_ref, *, shift):
    heads = within_ref.shape[1] // DK
    blocks = within_ref.shape[0] // CHUNK
    rows = pl.ds((lax.axis_index("tp") + shift) % blocks * CHUNK, CHUNK)
    for h in range(heads):
        cols = slice(h * DK, (h + 1) * DK)
        carried = dot_split((high_ref[rows, cols], low_ref[rows, cols]), halves(prior_ref[cols, :]))
        recurrent = within_ref[rows, cols] + carried
        square = jnp.mean(recurrent * recurrent, axis=1, keepdims=True)
        out_ref[:, cols] = (recurrent * lax.rsqrt(square + 1e-06) * gates_ref[rows, cols]).astype(BF16)


def gated_rows(shift, within, high, low, prior, gates):
    here = pl.BlockSpec(memory_space=pltpu.VMEM)
    return pl.pallas_call(
        functools.partial(readout_kernel, shift=shift),
        in_specs=[here] * 5,
        out_specs=here,
        out_shape=pltpu.VMEM((CHUNK, within.shape[1]), BF16),
        compiler_params=params(16),
        name="gated_rows",
    )(*map(in_vmem, (within, high, low, prior, gates)))


def slot_positions(routes, experts, capacity):
    rows = routes.shape[0]
    lanes = lax.broadcasted_iota(jnp.int32, (rows, experts), 1)
    first, second = (routes[:, 0:1], routes[:, 1:2])
    one, two = (lanes == first, lanes == second)
    named = (one.astype(F32) + two.astype(F32)).astype(BF16)
    earlier = dot_nn(lower_mask(rows, True).astype(BF16), named)
    ranks = [
        jnp.sum(jnp.where(hit, earlier, 0.0), axis=1, keepdims=True).astype(jnp.int32)
        for hit in (one, two)
    ]
    return [expert * (2 * capacity) + rank for expert, rank in zip((first, second), ranks)]


def slots_kernel(routes_ref, select_ref, pick_ref, *, experts, capacity):
    rows = routes_ref.shape[0]
    slots = 2 * experts * capacity
    places = slot_positions(routes_ref[...], experts, capacity)
    lanes = lax.broadcasted_iota(jnp.int32, (rows, slots), 1)
    down = lax.broadcasted_iota(jnp.int32, (slots, rows), 0)
    across = [
        jnp.transpose(jnp.broadcast_to(place.astype(F32), (rows, rows)))[0:1, :].astype(jnp.int32)
        for place in places
    ]
    for j in range(2):
        hit = (down == across[0] + j * capacity) | (down == across[1] + j * capacity)
        select_ref[:, j * rows : (j + 1) * rows] = jnp.where(hit, 1.0, 0.0).astype(BF16)
        for k in range(2):
            at = (2 * j + k) * rows
            pick_ref[at : at + rows, :] = jnp.where(lanes == places[k] + j * capacity, 1.0, 0.0).astype(BF16)


def slots_of(routes, experts, capacity):
    rows = routes.shape[0]
    slots = 2 * experts * capacity
    return pl.pallas_call(
        functools.partial(slots_kernel, experts=experts, capacity=capacity),
        out_shape=[pltpu.HBM((slots, 2 * rows), BF16), pltpu.HBM((4 * rows, slots), BF16)],
        compiler_params=params(12),
        name="slots_of",
    )(routes)


def own_kernel(own_ref, matrix_ref, resid_ref, select_ref, total_ref, matrix_out_ref, select_out_ref, sems):
    place = lax.axis_index("tp")
    inner = own_ref.shape[1]
    parts = sems.shape[0] - 1
    copies = []
    for k in range(parts):
        at = pl.ds((place + k) % parts * inner, inner)
        copies.append(pltpu.make_async_copy(matrix_ref.at[at, :], matrix_out_ref.at[at, :], sems.at[k]))
    copies.append(pltpu.make_async_copy(select_ref, select_out_ref, sems.at[parts]))
    for copy in copies:
        copy.start()
    copies[0].wait()
    part = dot_nn(own_ref[...], matrix_out_ref[pl.ds(place * inner, inner), :])
    total_ref[...] = resid_ref[...].astype(F32) + part
    for copy in copies[1:]:
        copy.wait()


def project_own(own, matrix, resid, select):
    rows = own.shape[0]
    here = pl.BlockSpec(memory_space=pltpu.VMEM)
    there = pl.BlockSpec(memory_space=pl.ANY)
    return pl.pallas_call(
        own_kernel,
        in_specs=[here, there, here, there],
        out_specs=[here, here, here],
        out_shape=[
            pltpu.VMEM((rows, matrix.shape[1]), F32),
            pltpu.VMEM(matrix.shape, BF16),
            pltpu.VMEM(select.shape, BF16),
        ],
        scratch_shapes=[pltpu.SemaphoreType.DMA((matrix.shape[0] // own.shape[1] + 1,))],
        compiler_params=params(16),
        name="project_own",
    )(in_vmem(own), in_hbm(matrix), in_vmem(resid), in_hbm(select))


def add_part(total, part_ref, matrix_ref, shift):
    inner = part_ref.shape[1]
    parts = matrix_ref.shape[0] // inner
    source = (lax.axis_index("tp") + parts - shift) % parts
    return total + dot_nn(part_ref[...], matrix_ref[pl.ds(source * inner, inner), :])


def more_kernel(part_ref, matrix_ref, total_ref, out_ref, *, shift):
    out_ref[...] = add_part(total_ref[...], part_ref, matrix_ref, shift)


def project_more(part, shift, matrix, total):
    here = pl.BlockSpec(memory_space=pltpu.VMEM)
    return pl.pallas_call(
        functools.partial(more_kernel, shift=shift),
        in_specs=[here, here, here],
        out_specs=here,
        out_shape=pltpu.VMEM(total.shape, F32),
        compiler_params=params(16),
        name="project_more",
    )(*map(in_vmem, (part, matrix, total)))


def project_kernel(part_ref, matrix_ref, total_ref, scale_ref, select_ref, stream_ref, packed_ref, stream_out, stacked, sem, *, shift):
    stream = add_part(total_ref[...], part_ref, matrix_ref, shift).astype(BF16)
    stream_out[...] = stream
    stream_copy = pltpu.make_async_copy(stream_out, stream_ref, sem)
    stream_copy.start()
    values = stream.astype(F32)
    square = jnp.mean(values * values, axis=1, keepdims=True)
    normed = (values * lax.rsqrt(square + 1e-06) * scale_ref[...]).astype(BF16)
    rows = normed.shape[0]
    half = normed.shape[1] // 2
    stacked[0:rows, :] = normed[:, :half]
    stacked[rows : 2 * rows, :] = normed[:, half:]
    packed_ref[...] = dot_nn(select_ref[...], stacked[...]).astype(BF16)
    stream_copy.wait()


def project(part, shift, matrix, total, scale, select):
    rows, width = total.shape
    slots = select.shape[0]
    here = pl.BlockSpec(memory_space=pltpu.VMEM)
    return pl.pallas_call(
        functools.partial(project_kernel, shift=shift),
        in_specs=[here, here, here, pl.BlockSpec((1, width), lambda: (0, 0)), here],
        out_specs=[pl.BlockSpec(memory_space=pl.ANY), here],
        scratch_shapes=[
            pltpu.VMEM((rows, width), BF16),
            pltpu.VMEM((2 * rows, width // 2), BF16),
            pltpu.SemaphoreType.DMA,
        ],
        out_shape=[pltpu.HBM((rows, width), BF16), pltpu.VMEM((slots, width // 2), BF16)],
        compiler_params=params(24),
        name="project",
    )(in_vmem(part), in_vmem(matrix), in_vmem(total), in_hbm(scale), in_vmem(select))


def expert_kernel(slots_ref, gate_ref, up_ref, down_ref, out_ref, rows_in, hidden, outs, sems):
    half = slots_ref.shape[1]
    split, rows2, wide = outs.shape
    rows = rows2 // 2
    cols = [slice(i * wide, (i + 1) * wide) for i in range(split)]
    out_copies = [pltpu.make_async_copy(outs.at[i], out_ref.at[:, cols[i]], sems.at[i]) for i in range(split)]
    group = 64
    upper = lax.broadcasted_iota(jnp.int32, (group // 16, 8, half), 1) < 4

    def untangle(i, carry):
        block = slots_ref[pl.ds(i * group, group), :].astype(F32).reshape(group // 16, 2, 8, half)
        one, two = (block[:, 0], block[:, 1])
        low = jnp.where(upper, one, pltpu.roll(two, 4, 1))
        high = jnp.where(upper, pltpu.roll(one, 4, 1), two)
        at = pl.ds(i * (group // 2), group // 2)
        rows_in[at, 0:half] = low.reshape(group // 2, half).astype(BF16)
        rows_in[at, half : 2 * half] = high.reshape(group // 2, half).astype(BF16)
        return carry

    lax.fori_loop(0, slots_ref.shape[0] // group, untangle, 0)

    for i in range(split):
        gates = dot_nn(rows_in[...], gate_ref[0, :, cols[i]])
        ups = dot_nn(rows_in[...], up_ref[0, :, cols[i]])
        hidden[:, cols[i]] = (gates / (1.0 + jnp.exp(-gates)) * ups).astype(BF16)

    top = lax.broadcasted_iota(jnp.int32, (rows // 8, 8, wide), 1) < 4
    for i in range(split):
        low = dot_nn(hidden[...], down_ref[0, :, cols[i]]).reshape(-1, 8, wide)
        high = dot_nn(hidden[...], down_ref[0, :, half + i * wide : half + (i + 1) * wide]).reshape(-1, 8, wide)
        one = jnp.where(top, low, pltpu.roll(high, 4, 1))
        two = jnp.where(top, pltpu.roll(low, 4, 1), high)
        outs[i] = jnp.stack([one, two], axis=1).reshape(2 * rows, wide).astype(BF16)
        out_copies[i].start()
    for i in range(split):
        out_copies[i].wait()


def experts_on(slots, gate_matrix, up_matrix, down_matrix):
    rows, half = slots.shape
    width, inner = gate_matrix.shape[1:]
    split = 4
    here = pl.BlockSpec(memory_space=pltpu.VMEM)
    return pl.pallas_call(
        expert_kernel,
        in_specs=[here, here, here, here],
        out_specs=pl.BlockSpec(memory_space=pl.ANY),
        out_shape=pltpu.HBM((rows, half), BF16),
        scratch_shapes=[
            pltpu.VMEM((rows // 2, width), BF16),
            pltpu.VMEM((rows // 2, inner), BF16),
            pltpu.VMEM((split, rows, half // split), BF16),
            pltpu.SemaphoreType.DMA((split,)),
        ],
        compiler_params=params(24),
        name="experts_on",
    )(*map(in_vmem, (slots, gate_matrix, up_matrix, down_matrix)))


def combine_kernel(returned_ref, pick_ref, weight_ref, stream_ref, out_ref, stream_in, outs, sems):
    rows, _ = stream_in.shape
    half = returned_ref.shape[1]
    stream_copy = pltpu.make_async_copy(stream_ref, stream_in, sems.at[0])
    stream_copy.start()
    weights = weight_ref[...]
    wide = outs.shape[2]
    copies = []
    for n in range(half // wide):
        picked = dot_nn(pick_ref[...], returned_ref[:, n * wide : (n + 1) * wide])
        if n == 0:
            stream_copy.wait()
        for j in range(2):
            at = 2 * j * rows
            cols = slice(j * half + n * wide, j * half + (n + 1) * wide)
            added = weights[:, 0:1] * picked[at : at + rows] + weights[:, 1:2] * picked[at + rows : at + 2 * rows]
            slot = 2 * n + j
            outs[slot] = (stream_in[:, cols].astype(F32) + added).astype(BF16)
            copies.append(pltpu.make_async_copy(outs.at[slot], out_ref.at[:, cols], sems.at[slot + 1]))
            copies[-1].start()
    for copy in copies:
        copy.wait()


def combine(returned, pick, stream, routing_weight):
    rows, width = stream.shape
    here = pl.BlockSpec(memory_space=pltpu.VMEM)
    there = pl.BlockSpec(memory_space=pl.ANY)
    pieces = 8
    return pl.pallas_call(
        combine_kernel,
        in_specs=[here, here, here, there],
        out_specs=there,
        out_shape=pltpu.HBM(stream.shape, BF16),
        scratch_shapes=[
            pltpu.VMEM((rows, width), BF16),
            pltpu.VMEM((pieces, rows, width // pieces), BF16),
            pltpu.SemaphoreType.DMA((pieces + 1,)),
        ],
        compiler_params=params(24),
        name="combine",
    )(in_vmem(returned), in_vmem(pick), in_vmem(routing_weight), in_hbm(stream))


def body(
    resid,
    query,
    forget_logits,
    forget_margin,
    decay_spike,
    value_logits,
    output_gate_logits,
    head_norm_scale,
    output_matrix,
    norm_scale_vector,
    routes,
    routing_weight,
    gate_matrix,
    up_matrix,
    down_matrix,
):
    rows, top = routes.shape
    experts = lax.axis_size(SP) * lax.axis_size("tp")
    capacity = 2 * rows * top // experts
    width = resid.shape[1]
    margin = forget_margin[None, :]
    places = lax.axis_size("tp")
    cum, values, start, sent = local_states(forget_logits, value_logits, margin, decay_spike.T)
    select, pick = slots_of(routes, experts, capacity)
    parts = lax.all_to_all(sent, SP, split_axis=0, concat_axis=0, tiled=True)
    within, high, low, gates = within_blocks(
        query, forget_logits, margin, cum, values, start, output_gate_logits, head_norm_scale[None, :]
    )
    prior = lax.all_to_all(carried_in(parts), SP, split_axis=0, concat_axis=0, tiled=True)
    prior = prior.reshape(start.shape[1], DK)
    shifts = (2, 1, places - 1)
    arrived = []
    for k in shifts + (0,):
        gated = gated_rows(k, within, high, low, prior, gates)
        if k:
            arrived.append(lax.ppermute(gated, "tp", [(i, (i + k) % places) for i in range(places)]))
    total, matrix, select = project_own(gated, output_matrix, resid, select)
    total = project_more(arrived[0], shifts[0], matrix, total)
    total = project_more(arrived[1], shifts[1], matrix, total)
    stream, packed = project(arrived[2], shifts[2], matrix, total, norm_scale_vector[None, :], select)
    shape = (experts, 2 * capacity, width // 2)
    slots = lax.all_to_all(packed.reshape(shape), SP_TP, split_axis=0, concat_axis=0, tiled=True)
    answers = experts_on(slots.reshape(packed.shape), gate_matrix, up_matrix, down_matrix)
    returned = lax.all_to_all(answers.reshape(shape), SP_TP, split_axis=0, concat_axis=0, tiled=True)
    return combine(returned.reshape(packed.shape), pick, stream, routing_weight)


def solution(mesh):
    finer = Mesh(mesh.devices.reshape(4, 4, 2, mesh.shape["tp"]), SP_TP)
    placed = (
        P(SP_TP, None),
        P(SP, "tp"),
        P(SP, "tp"),
        P("tp"),
        P(SP, "tp"),
        P(SP, "tp"),
        P(SP, "tp"),
        P("tp"),
        P(),
        P(),
        P(SP_TP, None),
        P(SP_TP, None),
        P(SP_TP, None, None),
        P(SP_TP, None, None),
        P(SP_TP, None, None),
    )
    return jax.shard_map(
        body, mesh=finer, in_specs=placed, out_specs=P(SP_TP, None), check_vma=False
    )
```

time: 143 us -> 140 us (0.979)
  Pallas kernels: 38.8 us -> 36.2 us
  waiting for transfers between devices: 36.9 us -> 35.1 us
    ppermute x3, waiting for transfers between devices: 2.81 us -> 0.01 us  [body(): lax.ppermute(gated, 'tp', [(i, (i + k) % places) for i in range(places)])]
    pallas_call x5 -> x11, Pallas kernels: 27.2 us -> 25.6 us  [the longest x1 8.21 us: experts_on(): pl.pallas_call(expert_kernel, in_specs=[here, here, here, here], out_spec...]
  transfers between devices with their start and end apart: 5 -> 5, of which waited for: 3 -> 2; matrix products, arithmetic and copies ran while one was open for 0% -> 0% of each run, Pallas kernels for 6% -> 11%
where the time goes in v2:
time: 140 us; the launch traced here: 139 us
  blocking collectives  53.4 us (38%)
  Pallas kernels  36.2 us (26%)
  waiting for transfers between devices  35.1 us (25%)
  starting transfers between devices  13.1 us (9%)
    all_to_all x1, blocking collectives, body(): lax.all_to_all(packed.reshape(shape), SP_TP, split_axis=0, concat_axis=0,...  34.9 us
    all_to_all x1, waiting for transfers between devices, body(): lax.all_to_all(answers.reshape(shape), SP_TP, split_axis=0, concat_axis=0...  30.8 us
    all_to_all x1, blocking collectives, body(): parts = lax.all_to_all(sent, SP, split_axis=0, concat_axis=0, tiled=True)  18.5 us
    pallas_call x1, Pallas kernels, experts_on(): pl.pallas_call(expert_kernel, in_specs=[here, here, here, here], out_spec...  8.21 us
    ppermute x3, starting transfers between devices, body(): lax.ppermute(gated, 'tp', [(i, (i + k) % places) for i in range(places)])  5.42 us
    pallas_call x1, Pallas kernels, local_states(): pl.pallas_call(state_kernel, grid=(STATE_STEPS,), in_specs=[pl.BlockSpec(...  5.23 us
    pallas_call x1, Pallas kernels, within_blocks(): pl.pallas_call(within_kernel, grid=(rows // CHUNK,), in_specs=[block, blo...  4.56 us
    all_to_all x1, waiting for transfers between devices, body(): lax.all_to_all(carried_in(parts), SP, split_axis=0, concat_axis=0, tiled=...  4.33 us
  transfers between devices with their start and end apart: 5, of which 2 were waited for; matrix products, arithmetic and copies ran while one was open for 0% of the time, Pallas kernels for 11%

profile of v2, /device:TPU:1, one launch (start us, length us, event | category | flops | bytes accessed | tf_op | source)
XLA Modules:
  0.0 139.5 jit_solution(16582201983029811717)
XLA Ops:
  0.0 5.2 %local_states.1 = (f32[512,512]{1,0:T(8,128)}, bf16[512,512]{1,0:T(8,128)(2,1)}, f32[4,512,128]{2,1,0:T(8,128)}, bf16[32,32,128]{2,1,0:T(8,128)(2,1)}) custom-call(bf16[512,512]{1,0:T(8,128)(2,1)} %forget_ref.3, bf16[512,512]{1,0:T(8,128)(2,1)} %value_ref.1, f32[1,512]{1,0:T(1,128)} %bitcast.17, f32[4,512]{1,0:T(4,128)} %bitcast.19), custom_call_target="tpu_custom_call" | custom-call | tf_op jit(solution)/shard_map/local_states/pallas_call | solution.py:105
  5.2 18.5 %all_to_all.20.parts_ref = bf16[32,32,128]{2,1,0:T(8,128)(2,1)S(1)} all-to-all(bf16[32,32,128]{2,1,0:T(8,128)(2,1)} %get-tuple-element.26), channel_id=1, replica_groups=mesh['sp_0'=4,'sp_1'=4,'sp_2'=2,'tp'=4] {'sp_0','sp_1','sp_2'}, dimensions={0} | all-to-all | bytes 524288 | tf_op jit(solution)/shard_map/all_to_all | solution.py:486
  23.7 0.8 carried_in.1
  24.5 3.8 %all-to-all-start.1 = ((f32[32,16,128]{2,1,0:T(8,128)}), f32[32,16,128]{2,1,0:T(8,128)S(1)}, u32[]{:S(2)}, u32[]{:S(2)}) async-start(f32[32,16,128]{2,1,0:T(8,128)} %carried_in.1), calls=%async_computation.1 | async-start | bytes 524288 | tf_op jit(solution)/shard_map/all_to_all | solution.py:490
  28.3 4.6 %within_blocks.1 = (f32[512,512]{1,0:T(8,128)S(1)}, bf16[512,512]{1,0:T(8,128)(2,1)S(1)}, bf16[512,512]{1,0:T(8,128)(2,1)S(1)}, f32[512,512]{1,0:T(8,128)S(1)}) custom-call(bf16[512,512]{1,0:T(8,128)(2,1)} %query_ref.1, bf16[512,512]{1,0:T(8,128)(2,1)} %forget_ref.3, f32[1,512]{1,0:T(1,128)} %bitcast.18, f32[512,512]{1,0:T(8,128)} %get-tuple-element.20.cum_ref, ...), custom_call_target="tpu_custom_call" | custom-call | tf_op jit(solution)/shard_map/within_blocks/pallas_call | solution.py:184
  32.8 4.3 %all-to-all-done.1 = f32[32,16,128]{2,1,0:T(8,128)S(1)} async-done(((f32[32,16,128]{2,1,0:T(8,128)}), f32[32,16,128]{2,1,0:T(8,128)S(1)}, u32[]{:S(2)}, u32[]{:S(2)}) %all-to-all-start.1) | async-done | bytes 262176 | tf_op jit(solution)/shard_map/all_to_all | solution.py:490
  37.2 1.2 gated_rows.7
  38.3 2.7 %collective-permute-start.2 = (bf16[128,512]{1,0:T(8,128)(2,1)}, bf16[128,512]{1,0:T(8,128)(2,1)}, u32[]{:S(2)}, u32[]{:S(2)}) collective-permute-start(bf16[128,512]{1,0:T(8,128)(2,1)} %gated_rows.7), channel_id=1, source_target_pairs={{0,2},{1,3},{2,0},{3,1},{4,6},{5,7},{6,4},{7,5},{8,10},{9,11},{10,... | collective-permute-start | bytes 393224 | tf_op jit(solution)/shard_map/ppermute | solution.py:497
  41.1 1.2 gated_rows.6
  42.2 0.3 collective-permute-start.1
  42.5 1.2 gated_rows.4
  43.7 2.4 %collective-permute-start = (bf16[128,512]{1,0:T(8,128)(2,1)}, bf16[128,512]{1,0:T(8,128)(2,1)}, u32[]{:S(2)}, u32[]{:S(2)}) collective-permute-start(bf16[128,512]{1,0:T(8,128)(2,1)} %gated_rows.4), channel_id=1, source_target_pairs={{0,3},{1,0},{2,1},{3,2},{4,7},{5,4},{6,5},{7,6},{8,11},{9,8},{10,9... | collective-permute-start | bytes 393224 | tf_op jit(solution)/shard_map/ppermute | solution.py:497
  46.0 0.1 copy.16.routes_ref
  46.2 1.8 %slots_of.1 = (bf16[1024,256]{1,0:T(8,128)(2,1)}, bf16[512,1024]{1,0:T(8,128)(2,1)}) custom-call(s32[128,2]{1,0:T(8,128)S(1)} %copy.16.routes_ref), custom_call_target="tpu_custom_call" | custom-call | tf_op jit(solution)/shard_map/slots_of/pallas_call | solution.py:255
  48.0 0.5 gated_rows.5.own_ref
  48.5 0.0 copy-start.4
  48.5 1.0 copy-done.4
  49.5 3.5 %project_own.1 = (f32[128,2048]{1,0:T(8,128)S(1)}, bf16[2048,2048]{1,0:T(8,128)(2,1)S(1)}, bf16[1024,256]{1,0:T(8,128)(2,1)S(1)}) custom-call(bf16[128,512]{1,0:T(8,128)(2,1)S(1)} %gated_rows.5.own_ref, bf16[2048,2048]{1,0:T(8,128)(2,1)} %matrix_ref.1, bf16[128,2048]{1,0:T(8,128)(2,1)S(1)} %copy-done.4, bf16[1024,256]{1,0:T(8,128)(2,1)} %get-tuple-element.28.select_ref), custom_call_target="tpu_custom_call" | custom-call | tf_op jit(solution)/shard_map/project_own/pallas_call | solution.py:285
  53.1 0.0 collective-permute-done.2.part_ref
  53.1 1.4 project_more.2.total_ref
  54.5 1.4 project_more.3.total_ref
  55.8 0.0 copy-start.1
  55.8 0.0 copy-start.2
  55.9 2.4 %project.1 = (bf16[128,2048]{1,0:T(8,128)(2,1)}, bf16[1024,1024]{1,0:T(8,128)(2,1)S(1)}) custom-call(bf16[128,512]{1,0:T(8,128)(2,1)} %collective-permute-done.part_ref, bf16[2048,2048]{1,0:T(8,128)(2,1)S(1)} %get-tuple-element.29.matrix_ref, f32[128,2048]{1,0:T(8,128)S(1)} %project_more.3.total_ref, f32[1,2048]{1,0:T(1,128)} %bitcast.20, ...), custom_call_target="tpu_custom_call" | custom-call | tf_op jit(solution)/shard_map/project/pallas_call | solution.py:343
  58.2 0.0 copy-start
  58.3 34.9 %all_to_all.21 = bf16[128,8,1024]{2,1,0:T(8,128)(2,1)S(1)} all-to-all(bf16[128,8,1024]{2,1,0:T(8,128)(2,1)S(1)} %bitcast.15), channel_id=1, replica_groups=mesh['sp_0'=4,'sp_1'=4,'sp_2'=2,'tp'=4] {'sp_0','sp_1','sp_2','tp'}, dimensions={0} | all-to-all | bytes 4194304 | tf_op jit(solution)/shard_map/all_to_all | solution.py:503
  93.2 8.2 %experts_on.1 = bf16[1024,1024]{1,0:T(8,128)(2,1)} custom-call(bf16[1024,1024]{1,0:T(8,128)(2,1)S(1)} %bitcast.10, bf16[1,2048,1024]{2,1,0:T(8,128)(2,1)S(1)} %copy-done, bf16[1,2048,1024]{2,1,0:T(8,128)(2,1)S(1)} %copy-done.1, bf16[1,1024,2048]{2,1,0:T(8,128)(2,1)S(1)} %copy-done.2), custom_call_target="tpu_custom_call" | custom-call | tf_op jit(solution)/shard_map/experts_on/pallas_call | solution.py:401
  101.4 0.0 copy-start.6
  101.4 3.9 %all-to-all-start.3 = ((bf16[128,8,1024]{2,1,0:T(8,128)(2,1)}), bf16[128,8,1024]{2,1,0:T(8,128)(2,1)S(1)}, u32[]{:S(2)}, u32[]{:S(2)}) async-start(bf16[128,8,1024]{2,1,0:T(8,128)(2,1)} %bitcast.16), calls=%async_computation.3 | async-start | bytes 4194304 | tf_op jit(solution)/shard_map/all_to_all | solution.py:505
  105.4 0.1 copy.17.weight_ref
  105.5 30.8 %all-to-all-done.3 = bf16[128,8,1024]{2,1,0:T(8,128)(2,1)S(1)} async-done(((bf16[128,8,1024]{2,1,0:T(8,128)(2,1)}), bf16[128,8,1024]{2,1,0:T(8,128)(2,1)S(1)}, u32[]{:S(2)}, u32[]{:S(2)}) %all-to-all-start.3) | async-done | bytes 2097184 | tf_op jit(solution)/shard_map/all_to_all | solution.py:505
  136.3 3.0 %combine.1 = bf16[128,2048]{1,0:T(8,128)(2,1)} custom-call(bf16[1024,1024]{1,0:T(8,128)(2,1)S(1)} %bitcast.9, bf16[512,1024]{1,0:T(8,128)(2,1)S(1)} %copy-done.3, f32[128,2]{1,0:T(8,128)S(1)} %copy.17.weight_ref, bf16[128,2048]{1,0:T(8,128)(2,1)} %get-tuple-element.34.stream_ref), custom_call_target="tpu_custom_call" | custom-call | tf_op jit(solution)/shard_map/combine/pallas_call | solution.py:446
  (10 shorter events, 0.0 us)
Async XLA Ops:
  24.5 12.7 %all-to-all-start.1 = ((f32[32,16,128]{2,1,0:T(8,128)}), f32[32,16,128]{2,1,0:T(8,128)S(1)}, u32[]{:S(2)}, u32[]{:S(2)}) async-start(f32[32,16,128]{2,1,0:T(8,128)} %carried_in.1), calls=%async_computation.1 | async-start | bytes 524288 | tf_op jit(solution)/shard_map/all_to_all | solution.py:490
  38.3 7.7 %copy-start.5 = (s32[128,2]{0,1:T(2,128)S(1)}, s32[128,2]{0,1:T(2,128)}, u32[]{:S(2)}) copy-start(s32[128,2]{0,1:T(2,128)} %param.25) | copy-start | bytes 3076
  38.3 14.8 %collective-permute-start.2 = (bf16[128,512]{1,0:T(8,128)(2,1)}, bf16[128,512]{1,0:T(8,128)(2,1)}, u32[]{:S(2)}, u32[]{:S(2)}) collective-permute-start(bf16[128,512]{1,0:T(8,128)(2,1)} %gated_rows.7), channel_id=1, source_target_pairs={{0,2},{1,3},{2,0},{3,1},{4,6},{5,7},{6,4},{7,5},{8,10},{9,11},{10,... | collective-permute-start | bytes 393224 | tf_op jit(solution)/shard_map/ppermute | solution.py:497
  42.2 12.2 %collective-permute-start.1 = (bf16[128,512]{1,0:T(8,128)(2,1)}, bf16[128,512]{1,0:T(8,128)(2,1)}, u32[]{:S(2)}, u32[]{:S(2)}) collective-permute-start(bf16[128,512]{1,0:T(8,128)(2,1)} %gated_rows.6), channel_id=1, source_target_pairs={{0,1},{1,2},{2,3},{3,0},{4,5},{5,6},{6,7},{7,4},{8,9},{9,10},{10,1... | collective-permute-start | bytes 393224 | tf_op jit(solution)/shard_map/ppermute | solution.py:497
  43.7 12.1 %collective-permute-start = (bf16[128,512]{1,0:T(8,128)(2,1)}, bf16[128,512]{1,0:T(8,128)(2,1)}, u32[]{:S(2)}, u32[]{:S(2)}) collective-permute-start(bf16[128,512]{1,0:T(8,128)(2,1)} %gated_rows.4), channel_id=1, source_target_pairs={{0,3},{1,0},{2,1},{3,2},{4,7},{5,4},{6,5},{7,6},{8,11},{9,8},{10,9... | collective-permute-start | bytes 393224 | tf_op jit(solution)/shard_map/ppermute | solution.py:497
  48.5 1.0 copy-start.4
  55.8 37.4 %copy-start.1 = (bf16[1,2048,1024]{2,1,0:T(8,128)(2,1)S(1)}, bf16[1,2048,1024]{2,1,0:T(8,128)(2,1)}, u32[]{:S(2)}) copy-start(bf16[1,2048,1024]{2,1,0:T(8,128)(2,1)} %up_ref.1) | copy-start | bytes 12582916
  55.8 37.4 %copy-start.2 = (bf16[1,1024,2048]{2,1,0:T(8,128)(2,1)S(1)}, bf16[1,1024,2048]{2,1,0:T(8,128)(2,1)}, u32[]{:S(2)}) copy-start(bf16[1,1024,2048]{2,1,0:T(8,128)(2,1)} %down_ref.1) | copy-start | bytes 12582916
  58.2 35.0 %copy-start = (bf16[1,2048,1024]{2,1,0:T(8,128)(2,1)S(1)}, bf16[1,2048,1024]{2,1,0:T(8,128)(2,1)}, u32[]{:S(2)}) copy-start(bf16[1,2048,1024]{2,1,0:T(8,128)(2,1)} %gate_ref.3) | copy-start | bytes 12582916
  101.4 4.0 %copy-start.6 = (f32[128,2]{0,1:T(2,128)S(1)}, f32[128,2]{0,1:T(2,128)}, u32[]{:S(2)}) copy-start(f32[128,2]{0,1:T(2,128)} %param.26) | copy-start | bytes 3076
  101.4 34.9 %copy-start.3 = (bf16[512,1024]{1,0:T(8,128)(2,1)S(1)}, bf16[512,1024]{1,0:T(8,128)(2,1)}, u32[]{:S(2)}) copy-start(bf16[512,1024]{1,0:T(8,128)(2,1)} %get-tuple-element.33.pick_ref) | copy-start | bytes 3145732
  101.4 34.8 %all-to-all-start.3 = ((bf16[128,8,1024]{2,1,0:T(8,128)(2,1)}), bf16[128,8,1024]{2,1,0:T(8,128)(2,1)S(1)}, u32[]{:S(2)}, u32[]{:S(2)}) async-start(bf16[128,8,1024]{2,1,0:T(8,128)(2,1)} %bitcast.16), calls=%async_computation.3 | async-start | bytes 4194304 | tf_op jit(solution)/shard_map/all_to_all | solution.py:505

commit v3 on v2

--- a/solution.py
+++ b/solution.py
@@ -46,12 +46,16 @@
     return pltpu.CompilerParams(vmem_limit_bytes=mebibytes * 1024 * 1024)
 
 
+def sigmoid(value):
+    return 1.0 / (1.0 + jnp.exp(-value))
+
+
 def halves(value):
     high = value.astype(BF16)
     return high, (value - high.astype(F32)).astype(BF16)
 
 
-def state_kernel(forget_ref, value_ref, margin_ref, spike_ref, cum_ref, values_ref, start_ref, sent_ref, state, before):
+def state_kernel(forget_ref, value_ref, margin_ref, spike_ref, cum_ref, values_ref, start_ref, sent_ref, state, before, keys_in, decays):
     step = pl.program_id(0)
     heads = forget_ref.shape[1] // DK
 
@@ -61,29 +65,37 @@
         before[...] = jnp.zeros_like(before)
 
     tri = lower_mask(CHUNK, False).astype(BF16)
-    for c in range(forget_ref.shape[0] // CHUNK):
-        rows = slice(c * CHUNK, (c + 1) * CHUNK)
-        spikes = halves(spike_ref[:, rows])
-        spikes = dot_nt(tri, spikes[0]) + dot_nt(tri, spikes[1])
+    tri = jnp.concatenate([tri, tri], axis=1)
+    blocks = [slice(c * CHUNK, (c + 1) * CHUNK) for c in range(forget_ref.shape[0] // CHUNK)]
+    for c, rows in enumerate(blocks):
+        for h in range(heads):
+            cols = slice(h * DK, (h + 1) * DK)
+            keys = margin_ref[:, cols] * sigmoid(-forget_ref[rows, cols].astype(F32))
+            keys_in[rows, cols] = keys
+            decays[c, 0:CHUNK, cols], decays[c, CHUNK : 2 * CHUNK, cols] = halves(jnp.log(1.0 - keys))
+    for c, rows in enumerate(blocks):
+        spikes = dot_nt(tri, jnp.concatenate(halves(spike_ref[:, rows]), axis=1))
+        sums = dot_nn(tri, decays[c])
+        for h in range(heads):
+            cols = slice(h * DK, (h + 1) * DK)
+            cum_ref[rows, cols] = sums[:, cols] + spikes[:, h : h + 1]
+    for c, rows in enumerate(blocks):
         start_ref[c] = state[...]
         for h in range(heads):
             cols = slice(h * DK, (h + 1) * DK)
-            keys = margin_ref[:, cols] / (1.0 + jnp.exp(forget_ref[rows, cols].astype(F32)))
-            high, low = halves(jnp.log(1.0 - keys))
-            cum = dot_nn(tri, high) + dot_nn(tri, low) + spikes[:, h : h + 1]
-            cum_ref[rows, cols] = cum
+            cum = cum_ref[rows, cols]
             last = cum[CHUNK - 1 : CHUNK, :]
             logits = value_ref[rows, cols].astype(F32)
-            values = (logits / (1.0 + jnp.exp(-logits))).astype(BF16)
+            values = (logits * sigmoid(logits)).astype(BF16)
             values_ref[rows, cols] = values
-            kept = (keys * jnp.exp(last - cum)).astype(BF16)
+            kept = (keys_in[rows, cols] * jnp.exp(last - cum)).astype(BF16)
             state[cols, :] = jnp.exp(last) * state[cols, :] + dot_tn(values, kept)
             before[:, cols] = before[:, cols] + last
 
     @pl.when(step == pl.num_programs(0) - 1)
     def _():
         share = DK // 8
-        first = lax.broadcasted_iota(jnp.int32, (share, DK), 0) == 0
+        first = lax.broadcasted_iota(jnp.int32, (TAIL, DK), 0) == 0
         for h in range(heads):
             total = before[:, h * DK : (h + 1) * DK]
             high = total.astype(BF16).astype(F32)
@@ -91,10 +103,11 @@
             for i in range(8):
                 row = h * DK + i * share
                 sent_ref[h * 8 + i, 0:share, :] = state[row : row + share, :].astype(BF16)
-                sent_ref[h * 8 + i, share : 2 * share, :] = tail
+                sent_ref[h * 8 + i, share : share + TAIL, :] = tail
 
 
 STATE_STEPS = 2
+TAIL = 8
 
 
 def local_states(forget_logits, value_logits, margin, spike):
@@ -115,15 +128,20 @@
             pl.BlockSpec((size, width), by_rows),
             pl.BlockSpec((size, width), by_rows),
             pl.BlockSpec((size // CHUNK, width, DK), lambda i: (i, 0, 0)),
-            pl.BlockSpec((heads * 8, 2 * DK // 8, DK), lambda i: (0, 0, 0)),
+            pl.BlockSpec((heads * 8, DK // 8 + TAIL, DK), lambda i: (0, 0, 0)),
         ],
         out_shape=[
             pltpu.HBM((rows, width), F32),
             pltpu.HBM((rows, width), BF16),
             pltpu.HBM((rows // CHUNK, width, DK), F32),
-            pltpu.HBM((heads * 8, 2 * DK // 8, DK), BF16),
-        ],
-        scratch_shapes=[pltpu.VMEM((width, DK), F32), pltpu.VMEM((1, width), F32)],
+            pltpu.HBM((heads * 8, DK // 8 + TAIL, DK), BF16),
+        ],
+        scratch_shapes=[
+            pltpu.VMEM((width, DK), F32),
+            pltpu.VMEM((1, width), F32),
+            pltpu.VMEM((size, width), F32),
+            pltpu.VMEM((size // CHUNK, 2 * CHUNK, width), BF16),
+        ],
         compiler_params=params(16),
         name="local_states",
     )(*map(in_hbm, (forget_logits, value_logits, margin, spike)))
@@ -134,7 +152,7 @@
     running = jnp.zeros(prior_ref.shape[1:], F32)
     for d in range(parts_ref.shape[0]):
         prior_ref[d] = running
-        tail = parts_ref[d, share : 2 * share, :].astype(F32)
+        tail = parts_ref[d, share : share + TAIL, :].astype(F32)
         total = tail[0:1, :] + tail[1:2, :]
         running = jnp.exp(total) * running + parts_ref[d, 0:share, :].astype(F32)
 
@@ -142,7 +160,7 @@
 def carried_in(parts):
     return pl.pallas_call(
         carry_kernel,
-        out_shape=jax.ShapeDtypeStruct((parts.shape[0], parts.shape[1] // 2, parts.shape[2]), F32),
+        out_shape=pltpu.HBM((parts.shape[0], parts.shape[1] - TAIL, parts.shape[2]), F32),
         compiler_params=params(8),
         name="carried_in",
     )(parts)
@@ -164,7 +182,7 @@
         cols = slice(h * DK, (h + 1) * DK)
         cum = cum_ref[:, cols]
         spread = cum - cum[CHUNK // 2 - 1 : CHUNK // 2, :]
-        keys = margin_ref[:, cols] / (1.0 + jnp.exp(forget_ref[:, cols].astype(F32)))
+        keys = margin_ref[:, cols] * sigmoid(-forget_ref[:, cols].astype(F32))
         queries = query_ref[:, cols].astype(F32) * (DK**-0.5)
         scores = dot_nt((queries * jnp.exp(spread)).astype(BF16), (keys * jnp.exp(-spread)).astype(BF16))
         scores = jnp.where(causal, scores, 0.0).astype(BF16)
@@ -174,7 +192,7 @@
         high_ref[:, cols], low_ref[:, cols] = halves(decayed * jnp.exp(before[:, cols]))
         before[:, cols] = before[:, cols] + cum[CHUNK - 1 : CHUNK, :]
         logits = gate_ref[:, cols].astype(F32)
-        gates_ref[:, cols] = scale_ref[:, cols] * (logits / (1.0 + jnp.exp(-logits)))
+        gates_ref[:, cols] = scale_ref[:, cols] * (logits * sigmoid(logits))
 
 
 def within_blocks(query, forget_logits, margin, cum, values, start, gate_logits, scale):
@@ -193,7 +211,7 @@
     )(*map(in_hbm, (query, forget_logits, margin, cum, values, start, gate_logits, scale)))
 
 
-def readout_kernel(within_ref, high_ref, low_ref, prior_ref, gates_ref, out_ref, *, shift):
+def readout(within_ref, high_ref, low_ref, prior_ref, gates_ref, out_ref, shift):
     heads = within_ref.shape[1] // DK
     blocks = within_ref.shape[0] // CHUNK
     rows = pl.ds((lax.axis_index("tp") + shift) % blocks * CHUNK, CHUNK)
@@ -203,6 +221,10 @@
         recurrent = within_ref[rows, cols] + carried
         square = jnp.mean(recurrent * recurrent, axis=1, keepdims=True)
         out_ref[:, cols] = (recurrent * lax.rsqrt(square + 1e-06) * gates_ref[rows, cols]).astype(BF16)
+
+
+def readout_kernel(*refs, shift):
+    readout(*refs, shift)
 
 
 def gated_rows(shift, within, high, low, prior, gates):
@@ -260,9 +282,9 @@
     )(routes)
 
 
-def own_kernel(own_ref, matrix_ref, resid_ref, select_ref, total_ref, matrix_out_ref, select_out_ref, sems):
+def own_kernel(within_ref, high_ref, low_ref, prior_ref, gates_ref, matrix_ref, resid_ref, select_ref, total_ref, matrix_out_ref, select_out_ref, own, sems):
     place = lax.axis_index("tp")
-    inner = own_ref.shape[1]
+    inner = own.shape[1]
     parts = sems.shape[0] - 1
     copies = []
     for k in range(parts):
@@ -271,30 +293,34 @@
     copies.append(pltpu.make_async_copy(select_ref, select_out_ref, sems.at[parts]))
     for copy in copies:
         copy.start()
+    readout(within_ref, high_ref, low_ref, prior_ref, gates_ref, own, 0)
     copies[0].wait()
-    part = dot_nn(own_ref[...], matrix_out_ref[pl.ds(place * inner, inner), :])
+    part = dot_nn(own[...], matrix_out_ref[pl.ds(place * inner, inner), :])
     total_ref[...] = resid_ref[...].astype(F32) + part
     for copy in copies[1:]:
         copy.wait()
 
 
-def project_own(own, matrix, resid, select):
-    rows = own.shape[0]
+def project_own(within, high, low, prior, gates, matrix, resid, select):
     here = pl.BlockSpec(memory_space=pltpu.VMEM)
     there = pl.BlockSpec(memory_space=pl.ANY)
+    inner = within.shape[1]
     return pl.pallas_call(
         own_kernel,
-        in_specs=[here, there, here, there],
+        in_specs=[here, here, here, here, here, there, here, there],
         out_specs=[here, here, here],
         out_shape=[
-            pltpu.VMEM((rows, matrix.shape[1]), F32),
+            pltpu.VMEM(resid.shape, F32),
             pltpu.VMEM(matrix.shape, BF16),
             pltpu.VMEM(select.shape, BF16),
         ],
-        scratch_shapes=[pltpu.SemaphoreType.DMA((matrix.shape[0] // own.shape[1] + 1,))],
+        scratch_shapes=[
+            pltpu.VMEM((CHUNK, inner), BF16),
+            pltpu.SemaphoreType.DMA((matrix.shape[0] // inner + 1,)),
+        ],
         compiler_params=params(16),
         name="project_own",
-    )(in_vmem(own), in_hbm(matrix), in_vmem(resid), in_hbm(select))
+    )(*map(in_vmem, (within, high, low, prior, gates)), in_hbm(matrix), in_vmem(resid), in_hbm(select))
 
 
 def add_part(total, part_ref, matrix_ref, shift):
@@ -442,7 +468,7 @@
     rows, width = stream.shape
     here = pl.BlockSpec(memory_space=pltpu.VMEM)
     there = pl.BlockSpec(memory_space=pl.ANY)
-    pieces = 8
+    pieces = 4
     return pl.pallas_call(
         combine_kernel,
         in_specs=[here, here, here, there],
@@ -491,11 +517,10 @@
     prior = prior.reshape(start.shape[1], DK)
     shifts = (2, 1, places - 1)
     arrived = []
-    for k in shifts + (0,):
+    for k in shifts:
         gated = gated_rows(k, within, high, low, prior, gates)
-        if k:
-            arrived.append(lax.ppermute(gated, "tp", [(i, (i + k) % places) for i in range(places)]))
-    total, matrix, select = project_own(gated, output_matrix, resid, select)
+        arrived.append(lax.ppermute(gated, "tp", [(i, (i + k) % places) for i in range(places)]))
+    total, matrix, select = project_own(within, high, low, prior, gates, output_matrix, resid, select)
     total = project_more(arrived[0], shifts[0], matrix, total)
     total = project_more(arrived[1], shifts[1], matrix, total)
     stream, packed = project(arrived[2], shifts[2], matrix, total, norm_scale_vector[None, :], select)

time: 140 us -> 137 us (0.979)
  Pallas kernels: 36.2 us -> 34.1 us
    pallas_call x4 -> x3, Pallas kernels: 3.97 us -> 3.47 us  [gated_rows(): pl.pallas_call(functools.partial(readout_kernel, shift=shift), in_specs=[...]
where the time goes in v3:
time: 137 us
  blocking collectives  52.8 us (39%)
  waiting for transfers between devices  35.1 us (26%)
  Pallas kernels  34.1 us (25%)
  starting transfers between devices  13.2 us (10%)
    all_to_all x1, blocking collectives, body(): lax.all_to_all(packed.reshape(shape), SP_TP, split_axis=0, concat_axis=0,...  34.9 us
    all_to_all x1, waiting for transfers between devices, body(): lax.all_to_all(answers.reshape(shape), SP_TP, split_axis=0, concat_axis=0...  30.8 us
    all_to_all x1, blocking collectives, body(): parts = lax.all_to_all(sent, SP, split_axis=0, concat_axis=0, tiled=True)  17.8 us
    pallas_call x1, Pallas kernels, experts_on(): pl.pallas_call(expert_kernel, in_specs=[here, here, here, here], out_spec...  8.21 us
    ppermute x3, starting transfers between devices, body(): lax.ppermute(gated, 'tp', [(i, (i + k) % places) for i in range(places)])  5.42 us
    pallas_call x1, Pallas kernels, within_blocks(): pl.pallas_call(within_kernel, grid=(rows // CHUNK,), in_specs=[block, blo...  4.58 us
    all_to_all x1, waiting for transfers between devices, body(): lax.all_to_all(carried_in(parts), SP, split_axis=0, concat_axis=0, tiled=...  4.29 us
    all_to_all x1, starting transfers between devices, body(): lax.all_to_all(answers.reshape(shape), SP_TP, split_axis=0, concat_axis=0...  3.94 us
  transfers between devices with their start and end apart: 5, of which 2 were waited for; matrix products, arithmetic and copies ran while one was open for 0% of the time, Pallas kernels for 11%

profile of v3, /device:TPU:1, one launch (start us, length us, event | category | flops | bytes accessed | tf_op | source)
XLA Modules:
  0.0 136.7 jit_solution(17560542811924223272)
XLA Ops:
  0.0 3.9 %local_states.1 = (f32[512,512]{1,0:T(8,128)}, bf16[512,512]{1,0:T(8,128)(2,1)}, f32[4,512,128]{2,1,0:T(8,128)}, bf16[32,24,128]{2,1,0:T(8,128)(2,1)}) custom-call(bf16[512,512]{1,0:T(8,128)(2,1)} %forget_ref.3, bf16[512,512]{1,0:T(8,128)(2,1)} %value_ref.1, f32[1,512]{1,0:T(1,128)} %bitcast.17, f32[4,512]{1,0:T(4,128)} %bitcast.19), custom_call_target="tpu_custom_call" | custom-call | tf_op jit(solution)/shard_map/local_states/pallas_call | solution.py:118
  3.9 17.8 %all_to_all.20.parts_ref = bf16[32,24,128]{2,1,0:T(8,128)(2,1)S(1)} all-to-all(bf16[32,24,128]{2,1,0:T(8,128)(2,1)} %get-tuple-element.26), channel_id=1, replica_groups=mesh['sp_0'=4,'sp_1'=4,'sp_2'=2,'tp'=4] {'sp_0','sp_1','sp_2'}, dimensions={0} | all-to-all | bytes 393216 | tf_op jit(solution)/shard_map/all_to_all | solution.py:512
  21.7 0.8 carried_in.1
  22.5 3.8 %all-to-all-start.1 = ((f32[32,16,128]{2,1,0:T(8,128)}), f32[32,16,128]{2,1,0:T(8,128)S(1)}, u32[]{:S(2)}, u32[]{:S(2)}) async-start(f32[32,16,128]{2,1,0:T(8,128)} %carried_in.1), calls=%async_computation.1 | async-start | bytes 524288 | tf_op jit(solution)/shard_map/all_to_all | solution.py:516
  26.3 4.6 %within_blocks.1 = (f32[512,512]{1,0:T(8,128)S(1)}, bf16[512,512]{1,0:T(8,128)(2,1)S(1)}, bf16[512,512]{1,0:T(8,128)(2,1)S(1)}, f32[512,512]{1,0:T(8,128)S(1)}) custom-call(bf16[512,512]{1,0:T(8,128)(2,1)} %query_ref.1, bf16[512,512]{1,0:T(8,128)(2,1)} %forget_ref.3, f32[1,512]{1,0:T(1,128)} %bitcast.18, f32[512,512]{1,0:T(8,128)} %get-tuple-element.20.cum_ref, ...), custom_call_target="tpu_custom_call" | custom-call | tf_op jit(solution)/shard_map/within_blocks/pallas_call | solution.py:202
  30.9 4.3 %all-to-all-done.1 = f32[32,16,128]{2,1,0:T(8,128)S(1)} async-done(((f32[32,16,128]{2,1,0:T(8,128)}), f32[32,16,128]{2,1,0:T(8,128)S(1)}, u32[]{:S(2)}, u32[]{:S(2)}) %all-to-all-start.1) | async-done | bytes 262176 | tf_op jit(solution)/shard_map/all_to_all | solution.py:516
  35.2 1.2 gated_rows.5
  36.4 2.7 %collective-permute-start.2 = (bf16[128,512]{1,0:T(8,128)(2,1)}, bf16[128,512]{1,0:T(8,128)(2,1)}, u32[]{:S(2)}, u32[]{:S(2)}) collective-permute-start(bf16[128,512]{1,0:T(8,128)(2,1)} %gated_rows.5), channel_id=1, source_target_pairs={{0,2},{1,3},{2,0},{3,1},{4,6},{5,7},{6,4},{7,5},{8,10},{9,11},{10,... | collective-permute-start | bytes 393224 | tf_op jit(solution)/shard_map/ppermute | solution.py:522
  39.1 1.2 gated_rows.4
  40.3 0.3 collective-permute-start.1
  40.6 1.2 gated_rows.3
  41.7 2.4 %collective-permute-start = (bf16[128,512]{1,0:T(8,128)(2,1)}, bf16[128,512]{1,0:T(8,128)(2,1)}, u32[]{:S(2)}, u32[]{:S(2)}) collective-permute-start(bf16[128,512]{1,0:T(8,128)(2,1)} %gated_rows.3), channel_id=1, source_target_pairs={{0,3},{1,0},{2,1},{3,2},{4,7},{5,4},{6,5},{7,6},{8,11},{9,8},{10,9... | collective-permute-start | bytes 393224 | tf_op jit(solution)/shard_map/ppermute | solution.py:522
  44.1 0.1 copy.16.routes_ref
  44.2 1.8 %slots_of.1 = (bf16[1024,256]{1,0:T(8,128)(2,1)}, bf16[512,1024]{1,0:T(8,128)(2,1)}) custom-call(s32[128,2]{1,0:T(8,128)S(1)} %copy.16.routes_ref), custom_call_target="tpu_custom_call" | custom-call | tf_op jit(solution)/shard_map/slots_of/pallas_call | solution.py:277
  46.0 1.0 copy-done.4
  47.1 3.8 %project_own.1 = (f32[128,2048]{1,0:T(8,128)S(1)}, bf16[2048,2048]{1,0:T(8,128)(2,1)S(1)}, bf16[1024,256]{1,0:T(8,128)(2,1)S(1)}) custom-call(f32[512,512]{1,0:T(8,128)S(1)} %get-tuple-element.23.refs_0_.within_ref, bf16[512,512]{1,0:T(8,128)(2,1)S(1)} %get-tuple-element.24.refs_1_.high_ref, bf16[512,512]{1,0:T(8,128)(2,1)S(1)} %get-tuple-element.25.refs_2_.low_ref, ...), custom_call_target="tpu_custom_call" | custom-call | tf_op jit(solution)/shard_map/project_own/pallas_call | solution.py:308
  50.9 0.0 collective-permute-done.2.part_ref
  50.9 1.4 project_more.2.total_ref
  52.2 0.0 collective-permute-done.1.part_ref
  52.2 1.4 project_more.3.total_ref
  53.6 0.0 collective-permute-done.part_ref
  53.6 0.0 copy-start.1
  53.6 0.0 copy-start.2
  53.6 2.4 %project.1 = (bf16[128,2048]{1,0:T(8,128)(2,1)}, bf16[1024,1024]{1,0:T(8,128)(2,1)S(1)}) custom-call(bf16[128,512]{1,0:T(8,128)(2,1)} %collective-permute-done.part_ref, bf16[2048,2048]{1,0:T(8,128)(2,1)S(1)} %get-tuple-element.29.matrix_ref, f32[128,2048]{1,0:T(8,128)S(1)} %project_more.3.total_ref, f32[1,2048]{1,0:T(1,128)} %bitcast.20, ...), custom_call_target="tpu_custom_call" | custom-call | tf_op jit(solution)/shard_map/project/pallas_call | solution.py:369
  56.0 0.0 copy-start
  56.0 34.9 %all_to_all.21 = bf16[128,8,1024]{2,1,0:T(8,128)(2,1)S(1)} all-to-all(bf16[128,8,1024]{2,1,0:T(8,128)(2,1)S(1)} %bitcast.15), channel_id=1, replica_groups=mesh['sp_0'=4,'sp_1'=4,'sp_2'=2,'tp'=4] {'sp_0','sp_1','sp_2','tp'}, dimensions={0} | all-to-all | bytes 4194304 | tf_op jit(solution)/shard_map/all_to_all | solution.py:528
  91.0 8.2 %experts_on.1 = bf16[1024,1024]{1,0:T(8,128)(2,1)} custom-call(bf16[1024,1024]{1,0:T(8,128)(2,1)S(1)} %bitcast.10, bf16[1,2048,1024]{2,1,0:T(8,128)(2,1)S(1)} %copy-done, bf16[1,2048,1024]{2,1,0:T(8,128)(2,1)S(1)} %copy-done.1, bf16[1,1024,2048]{2,1,0:T(8,128)(2,1)S(1)} %copy-done.2), custom_call_target="tpu_custom_call" | custom-call | tf_op jit(solution)/shard_map/experts_on/pallas_call | solution.py:427
  99.2 0.0 copy-start.6
  99.2 3.9 %all-to-all-start.3 = ((bf16[128,8,1024]{2,1,0:T(8,128)(2,1)}), bf16[128,8,1024]{2,1,0:T(8,128)(2,1)S(1)}, u32[]{:S(2)}, u32[]{:S(2)}) async-start(bf16[128,8,1024]{2,1,0:T(8,128)(2,1)} %bitcast.16), calls=%async_computation.3 | async-start | bytes 4194304 | tf_op jit(solution)/shard_map/all_to_all | solution.py:530
  103.2 0.1 copy.17.weight_ref
  103.3 30.8 %all-to-all-done.3 = bf16[128,8,1024]{2,1,0:T(8,128)(2,1)S(1)} async-done(((bf16[128,8,1024]{2,1,0:T(8,128)(2,1)}), bf16[128,8,1024]{2,1,0:T(8,128)(2,1)S(1)}, u32[]{:S(2)}, u32[]{:S(2)}) %all-to-all-start.3) | async-done | bytes 2097184 | tf_op jit(solution)/shard_map/all_to_all | solution.py:530
  134.1 2.5 %combine.1 = bf16[128,2048]{1,0:T(8,128)(2,1)} custom-call(bf16[1024,1024]{1,0:T(8,128)(2,1)S(1)} %bitcast.9, bf16[512,1024]{1,0:T(8,128)(2,1)S(1)} %copy-done.3, f32[128,2]{1,0:T(8,128)S(1)} %copy.17.weight_ref, bf16[128,2048]{1,0:T(8,128)(2,1)} %get-tuple-element.34.stream_ref), custom_call_target="tpu_custom_call" | custom-call | tf_op jit(solution)/shard_map/combine/pallas_call | solution.py:472
  (9 shorter events, 0.0 us)
Async XLA Ops:
  22.5 12.7 %all-to-all-start.1 = ((f32[32,16,128]{2,1,0:T(8,128)}), f32[32,16,128]{2,1,0:T(8,128)S(1)}, u32[]{:S(2)}, u32[]{:S(2)}) async-start(f32[32,16,128]{2,1,0:T(8,128)} %carried_in.1), calls=%async_computation.1 | async-start | bytes 524288 | tf_op jit(solution)/shard_map/all_to_all | solution.py:516
  36.4 7.7 %copy-start.5 = (s32[128,2]{0,1:T(2,128)S(1)}, s32[128,2]{0,1:T(2,128)}, u32[]{:S(2)}) copy-start(s32[128,2]{0,1:T(2,128)} %param.25) | copy-start | bytes 3076
  36.4 14.5 %collective-permute-start.2 = (bf16[128,512]{1,0:T(8,128)(2,1)}, bf16[128,512]{1,0:T(8,128)(2,1)}, u32[]{:S(2)}, u32[]{:S(2)}) collective-permute-start(bf16[128,512]{1,0:T(8,128)(2,1)} %gated_rows.5), channel_id=1, source_target_pairs={{0,2},{1,3},{2,0},{3,1},{4,6},{5,7},{6,4},{7,5},{8,10},{9,11},{10,... | collective-permute-start | bytes 393224 | tf_op jit(solution)/shard_map/ppermute | solution.py:522
  40.3 12.0 %collective-permute-start.1 = (bf16[128,512]{1,0:T(8,128)(2,1)}, bf16[128,512]{1,0:T(8,128)(2,1)}, u32[]{:S(2)}, u32[]{:S(2)}) collective-permute-start(bf16[128,512]{1,0:T(8,128)(2,1)} %gated_rows.4), channel_id=1, source_target_pairs={{0,1},{1,2},{2,3},{3,0},{4,5},{5,6},{6,7},{7,4},{8,9},{9,10},{10,1... | collective-permute-start | bytes 393224 | tf_op jit(solution)/shard_map/ppermute | solution.py:522
  41.7 11.9 %collective-permute-start = (bf16[128,512]{1,0:T(8,128)(2,1)}, bf16[128,512]{1,0:T(8,128)(2,1)}, u32[]{:S(2)}, u32[]{:S(2)}) collective-permute-start(bf16[128,512]{1,0:T(8,128)(2,1)} %gated_rows.3), channel_id=1, source_target_pairs={{0,3},{1,0},{2,1},{3,2},{4,7},{5,4},{6,5},{7,6},{8,11},{9,8},{10,9... | collective-permute-start | bytes 393224 | tf_op jit(solution)/shard_map/ppermute | solution.py:522
  46.0 1.0 copy-start.4
  53.6 37.4 %copy-start.1 = (bf16[1,2048,1024]{2,1,0:T(8,128)(2,1)S(1)}, bf16[1,2048,1024]{2,1,0:T(8,128)(2,1)}, u32[]{:S(2)}) copy-start(bf16[1,2048,1024]{2,1,0:T(8,128)(2,1)} %up_ref.1) | copy-start | bytes 12582916
  53.6 37.4 %copy-start.2 = (bf16[1,1024,2048]{2,1,0:T(8,128)(2,1)S(1)}, bf16[1,1024,2048]{2,1,0:T(8,128)(2,1)}, u32[]{:S(2)}) copy-start(bf16[1,1024,2048]{2,1,0:T(8,128)(2,1)} %down_ref.1) | copy-start | bytes 12582916
  56.0 35.0 %copy-start = (bf16[1,2048,1024]{2,1,0:T(8,128)(2,1)S(1)}, bf16[1,2048,1024]{2,1,0:T(8,128)(2,1)}, u32[]{:S(2)}) copy-start(bf16[1,2048,1024]{2,1,0:T(8,128)(2,1)} %gate_ref.3) | copy-start | bytes 12582916
  99.2 4.0 %copy-start.6 = (f32[128,2]{0,1:T(2,128)S(1)}, f32[128,2]{0,1:T(2,128)}, u32[]{:S(2)}) copy-start(f32[128,2]{0,1:T(2,128)} %param.26) | copy-start | bytes 3076
  99.2 34.9 %copy-start.3 = (bf16[512,1024]{1,0:T(8,128)(2,1)S(1)}, bf16[512,1024]{1,0:T(8,128)(2,1)}, u32[]{:S(2)}) copy-start(bf16[512,1024]{1,0:T(8,128)(2,1)} %get-tuple-element.33.pick_ref) | copy-start | bytes 3145732
  99.2 34.8 %all-to-all-start.3 = ((bf16[128,8,1024]{2,1,0:T(8,128)(2,1)}), bf16[128,8,1024]{2,1,0:T(8,128)(2,1)S(1)}, u32[]{:S(2)}, u32[]{:S(2)}) async-start(bf16[128,8,1024]{2,1,0:T(8,128)(2,1)} %bitcast.16), calls=%async_computation.3 | async-start | bytes 4194304 | tf_op jit(solution)/shard_map/all_to_all | solution.py:530

commit v4 on v3

--- a/solution.py
+++ b/solution.py
@@ -368,7 +368,7 @@
     here = pl.BlockSpec(memory_space=pltpu.VMEM)
     return pl.pallas_call(
         functools.partial(project_kernel, shift=shift),
-        in_specs=[here, here, here, pl.BlockSpec((1, width), lambda: (0, 0)), here],
+        in_specs=[here, here, here, here, here],
         out_specs=[pl.BlockSpec(memory_space=pl.ANY), here],
         scratch_shapes=[
             pltpu.VMEM((rows, width), BF16),
@@ -378,7 +378,7 @@
         out_shape=[pltpu.HBM((rows, width), BF16), pltpu.VMEM((slots, width // 2), BF16)],
         compiler_params=params(24),
         name="project",
-    )(in_vmem(part), in_vmem(matrix), in_vmem(total), in_hbm(scale), in_vmem(select))
+    )(*map(in_vmem, (part, matrix, total, scale, select)))
 
 
 def expert_kernel(slots_ref, gate_ref, up_ref, down_ref, out_ref, rows_in, hidden, outs, sems):
@@ -390,17 +390,14 @@
     group = 64
     upper = lax.broadcasted_iota(jnp.int32, (group // 16, 8, half), 1) < 4
 
-    def untangle(i, carry):
-        block = slots_ref[pl.ds(i * group, group), :].astype(F32).reshape(group // 16, 2, 8, half)
+    for i in range(slots_ref.shape[0] // group):
+        block = slots_ref[i * group : (i + 1) * group, :].astype(F32).reshape(group // 16, 2, 8, half)
         one, two = (block[:, 0], block[:, 1])
         low = jnp.where(upper, one, pltpu.roll(two, 4, 1))
         high = jnp.where(upper, pltpu.roll(one, 4, 1), two)
-        at = pl.ds(i * (group // 2), group // 2)
+        at = slice(i * (group // 2), (i + 1) * (group // 2))
         rows_in[at, 0:half] = low.reshape(group // 2, half).astype(BF16)
         rows_in[at, half : 2 * half] = high.reshape(group // 2, half).astype(BF16)
-        return carry
-
-    lax.fori_loop(0, slots_ref.shape[0] // group, untangle, 0)
 
     for i in range(split):
         gates = dot_nn(rows_in[...], gate_ref[0, :, cols[i]])

time: 137 us -> 137 us (level)
  no operation moved by 1% of the time
where the time goes in v4:
time: 137 us; the launch traced here: 136 us
  blocking collectives  52.8 us (39%)
  waiting for transfers between devices  35.1 us (26%)
  Pallas kernels  33.5 us (24%)
  starting transfers between devices  13.2 us (10%)
    all_to_all x1, blocking collectives, body(): lax.all_to_all(packed.reshape(shape), SP_TP, split_axis=0, concat_axis=0,...  34.9 us
    all_to_all x1, waiting for transfers between devices, body(): lax.all_to_all(answers.reshape(shape), SP_TP, split_axis=0, concat_axis=0...  30.8 us
    all_to_all x1, blocking collectives, body(): parts = lax.all_to_all(sent, SP, split_axis=0, concat_axis=0, tiled=True)  17.8 us
    pallas_call x1, Pallas kernels, experts_on(): pl.pallas_call(expert_kernel, in_specs=[here, here, here, here], out_spec...  7.57 us
    ppermute x3, starting transfers between devices, body(): lax.ppermute(gated, 'tp', [(i, (i + k) % places) for i in range(places)])  5.42 us
    pallas_call x1, Pallas kernels, within_blocks(): pl.pallas_call(within_kernel, grid=(rows // CHUNK,), in_specs=[block, blo...  4.58 us
    all_to_all x1, waiting for transfers between devices, body(): lax.all_to_all(carried_in(parts), SP, split_axis=0, concat_axis=0, tiled=...  4.29 us
    all_to_all x1, starting transfers between devices, body(): lax.all_to_all(answers.reshape(shape), SP_TP, split_axis=0, concat_axis=0...  3.94 us
  transfers between devices with their start and end apart: 5, of which 2 were waited for; matrix products, arithmetic and copies ran while one was open for 0% of the time, Pallas kernels for 11%

profile of v4, /device:TPU:1, one launch (start us, length us, event | category | flops | bytes accessed | tf_op | source)
XLA Modules:
  0.0 136.1 jit_solution(15875519423956461207)
XLA Ops:
  0.0 3.9 %local_states.1 = (f32[512,512]{1,0:T(8,128)}, bf16[512,512]{1,0:T(8,128)(2,1)}, f32[4,512,128]{2,1,0:T(8,128)}, bf16[32,24,128]{2,1,0:T(8,128)(2,1)}) custom-call(bf16[512,512]{1,0:T(8,128)(2,1)} %forget_ref.3, bf16[512,512]{1,0:T(8,128)(2,1)} %value_ref.1, f32[1,512]{1,0:T(1,128)} %bitcast.18, f32[4,512]{1,0:T(4,128)} %bitcast.20), custom_call_target="tpu_custom_call" | custom-call | tf_op jit(solution)/shard_map/local_states/pallas_call | solution.py:118
  3.9 17.8 %all_to_all.20.parts_ref = bf16[32,24,128]{2,1,0:T(8,128)(2,1)S(1)} all-to-all(bf16[32,24,128]{2,1,0:T(8,128)(2,1)} %get-tuple-element.26), channel_id=1, replica_groups=mesh['sp_0'=4,'sp_1'=4,'sp_2'=2,'tp'=4] {'sp_0','sp_1','sp_2'}, dimensions={0} | all-to-all | bytes 393216 | tf_op jit(solution)/shard_map/all_to_all | solution.py:509
  21.7 0.8 carried_in.1
  22.5 3.8 %all-to-all-start.1 = ((f32[32,16,128]{2,1,0:T(8,128)}), f32[32,16,128]{2,1,0:T(8,128)S(1)}, u32[]{:S(2)}, u32[]{:S(2)}) async-start(f32[32,16,128]{2,1,0:T(8,128)} %carried_in.1), calls=%async_computation.1 | async-start | bytes 524288 | tf_op jit(solution)/shard_map/all_to_all | solution.py:513
  26.3 4.6 %within_blocks.1 = (f32[512,512]{1,0:T(8,128)S(1)}, bf16[512,512]{1,0:T(8,128)(2,1)S(1)}, bf16[512,512]{1,0:T(8,128)(2,1)S(1)}, f32[512,512]{1,0:T(8,128)S(1)}) custom-call(bf16[512,512]{1,0:T(8,128)(2,1)} %query_ref.1, bf16[512,512]{1,0:T(8,128)(2,1)} %forget_ref.3, f32[1,512]{1,0:T(1,128)} %bitcast.19, f32[512,512]{1,0:T(8,128)} %get-tuple-element.20.cum_ref, ...), custom_call_target="tpu_custom_call" | custom-call | tf_op jit(solution)/shard_map/within_blocks/pallas_call | solution.py:202
  30.9 4.3 %all-to-all-done.1 = f32[32,16,128]{2,1,0:T(8,128)S(1)} async-done(((f32[32,16,128]{2,1,0:T(8,128)}), f32[32,16,128]{2,1,0:T(8,128)S(1)}, u32[]{:S(2)}, u32[]{:S(2)}) %all-to-all-start.1) | async-done | bytes 262176 | tf_op jit(solution)/shard_map/all_to_all | solution.py:513
  35.2 1.2 gated_rows.5
  36.3 2.7 %collective-permute-start.2 = (bf16[128,512]{1,0:T(8,128)(2,1)}, bf16[128,512]{1,0:T(8,128)(2,1)}, u32[]{:S(2)}, u32[]{:S(2)}) collective-permute-start(bf16[128,512]{1,0:T(8,128)(2,1)} %gated_rows.5), channel_id=1, source_target_pairs={{0,2},{1,3},{2,0},{3,1},{4,6},{5,7},{6,4},{7,5},{8,10},{9,11},{10,... | collective-permute-start | bytes 393224 | tf_op jit(solution)/shard_map/ppermute | solution.py:519
  39.1 1.1 gated_rows.4
  40.2 0.3 collective-permute-start.1
  40.5 1.2 gated_rows.3
  41.7 2.4 %collective-permute-start = (bf16[128,512]{1,0:T(8,128)(2,1)}, bf16[128,512]{1,0:T(8,128)(2,1)}, u32[]{:S(2)}, u32[]{:S(2)}) collective-permute-start(bf16[128,512]{1,0:T(8,128)(2,1)} %gated_rows.3), channel_id=1, source_target_pairs={{0,3},{1,0},{2,1},{3,2},{4,7},{5,4},{6,5},{7,6},{8,11},{9,8},{10,9... | collective-permute-start | bytes 393224 | tf_op jit(solution)/shard_map/ppermute | solution.py:519
  44.1 0.1 copy.16.routes_ref
  44.2 1.8 %slots_of.1 = (bf16[1024,256]{1,0:T(8,128)(2,1)}, bf16[512,1024]{1,0:T(8,128)(2,1)}) custom-call(s32[128,2]{1,0:T(8,128)S(1)} %copy.16.routes_ref), custom_call_target="tpu_custom_call" | custom-call | tf_op jit(solution)/shard_map/slots_of/pallas_call | solution.py:277
  46.0 1.0 copy-done.4
  47.0 3.8 %project_own.1 = (f32[128,2048]{1,0:T(8,128)S(1)}, bf16[2048,2048]{1,0:T(8,128)(2,1)S(1)}, bf16[1024,256]{1,0:T(8,128)(2,1)S(1)}) custom-call(f32[512,512]{1,0:T(8,128)S(1)} %get-tuple-element.23.refs_0_.within_ref, bf16[512,512]{1,0:T(8,128)(2,1)S(1)} %get-tuple-element.24.refs_1_.high_ref, bf16[512,512]{1,0:T(8,128)(2,1)S(1)} %get-tuple-element.25.refs_2_.low_ref, ...), custom_call_target="tpu_custom_call" | custom-call | tf_op jit(solution)/shard_map/project_own/pallas_call | solution.py:308
  50.8 1.4 project_more.2.total_ref
  52.2 0.0 copy-start.5
  52.2 0.0 collective-permute-done.1.part_ref
  52.2 1.4 project_more.3.total_ref
  53.6 0.0 collective-permute-done.part_ref
  53.6 0.0 copy-start.1
  53.6 0.0 copy-start.2
  53.6 2.4 %project.1 = (bf16[128,2048]{1,0:T(8,128)(2,1)}, bf16[1024,1024]{1,0:T(8,128)(2,1)S(1)}) custom-call(bf16[128,512]{1,0:T(8,128)(2,1)} %collective-permute-done.part_ref, bf16[2048,2048]{1,0:T(8,128)(2,1)S(1)} %get-tuple-element.29.matrix_ref, f32[128,2048]{1,0:T(8,128)S(1)} %project_more.3.total_ref, f32[1,2048]{1,0:T(1,128)S(1)} %bitcast.16, ...), custom_call_target="tpu_custom_call" | custom-call | tf_op jit(solution)/shard_map/project/pallas_call | solution.py:369
  56.0 0.0 copy-start
  56.0 34.9 %all_to_all.21 = bf16[128,8,1024]{2,1,0:T(8,128)(2,1)S(1)} all-to-all(bf16[128,8,1024]{2,1,0:T(8,128)(2,1)S(1)} %bitcast.15), channel_id=1, replica_groups=mesh['sp_0'=4,'sp_1'=4,'sp_2'=2,'tp'=4] {'sp_0','sp_1','sp_2','tp'}, dimensions={0} | all-to-all | bytes 4194304 | tf_op jit(solution)/shard_map/all_to_all | solution.py:525
  91.0 7.6 %experts_on.1 = bf16[1024,1024]{1,0:T(8,128)(2,1)} custom-call(bf16[1024,1024]{1,0:T(8,128)(2,1)S(1)} %bitcast.10, bf16[1,2048,1024]{2,1,0:T(8,128)(2,1)S(1)} %copy-done, bf16[1,2048,1024]{2,1,0:T(8,128)(2,1)S(1)} %copy-done.1, bf16[1,1024,2048]{2,1,0:T(8,128)(2,1)S(1)} %copy-done.2), custom_call_target="tpu_custom_call" | custom-call | tf_op jit(solution)/shard_map/experts_on/pallas_call | solution.py:424
  98.6 0.0 copy-start.7
  98.6 3.9 %all-to-all-start.3 = ((bf16[128,8,1024]{2,1,0:T(8,128)(2,1)}), bf16[128,8,1024]{2,1,0:T(8,128)(2,1)S(1)}, u32[]{:S(2)}, u32[]{:S(2)}) async-start(bf16[128,8,1024]{2,1,0:T(8,128)(2,1)} %bitcast.17), calls=%async_computation.3 | async-start | bytes 4194304 | tf_op jit(solution)/shard_map/all_to_all | solution.py:527
  102.6 0.1 copy.17.weight_ref
  102.7 30.8 %all-to-all-done.3 = bf16[128,8,1024]{2,1,0:T(8,128)(2,1)S(1)} async-done(((bf16[128,8,1024]{2,1,0:T(8,128)(2,1)}), bf16[128,8,1024]{2,1,0:T(8,128)(2,1)S(1)}, u32[]{:S(2)}, u32[]{:S(2)}) %all-to-all-start.3) | async-done | bytes 2097184 | tf_op jit(solution)/shard_map/all_to_all | solution.py:527
  133.5 2.5 %combine.1 = bf16[128,2048]{1,0:T(8,128)(2,1)} custom-call(bf16[1024,1024]{1,0:T(8,128)(2,1)S(1)} %bitcast.9, bf16[512,1024]{1,0:T(8,128)(2,1)S(1)} %copy-done.3, f32[128,2]{1,0:T(8,128)S(1)} %copy.17.weight_ref, bf16[128,2048]{1,0:T(8,128)(2,1)} %get-tuple-element.34.stream_ref), custom_call_target="tpu_custom_call" | custom-call | tf_op jit(solution)/shard_map/combine/pallas_call | solution.py:469
  (11 shorter events, 0.0 us)
Async XLA Ops:
  22.5 12.7 %all-to-all-start.1 = ((f32[32,16,128]{2,1,0:T(8,128)}), f32[32,16,128]{2,1,0:T(8,128)S(1)}, u32[]{:S(2)}, u32[]{:S(2)}) async-start(f32[32,16,128]{2,1,0:T(8,128)} %carried_in.1), calls=%async_computation.1 | async-start | bytes 524288 | tf_op jit(solution)/shard_map/all_to_all | solution.py:513
  36.3 7.7 %copy-start.6 = (s32[128,2]{0,1:T(2,128)S(1)}, s32[128,2]{0,1:T(2,128)}, u32[]{:S(2)}) copy-start(s32[128,2]{0,1:T(2,128)} %param.25) | copy-start | bytes 3076
  36.3 14.5 %collective-permute-start.2 = (bf16[128,512]{1,0:T(8,128)(2,1)}, bf16[128,512]{1,0:T(8,128)(2,1)}, u32[]{:S(2)}, u32[]{:S(2)}) collective-permute-start(bf16[128,512]{1,0:T(8,128)(2,1)} %gated_rows.5), channel_id=1, source_target_pairs={{0,2},{1,3},{2,0},{3,1},{4,6},{5,7},{6,4},{7,5},{8,10},{9,11},{10,... | collective-permute-start | bytes 393224 | tf_op jit(solution)/shard_map/ppermute | solution.py:519
  40.2 12.0 %collective-permute-start.1 = (bf16[128,512]{1,0:T(8,128)(2,1)}, bf16[128,512]{1,0:T(8,128)(2,1)}, u32[]{:S(2)}, u32[]{:S(2)}) collective-permute-start(bf16[128,512]{1,0:T(8,128)(2,1)} %gated_rows.4), channel_id=1, source_target_pairs={{0,1},{1,2},{2,3},{3,0},{4,5},{5,6},{6,7},{7,4},{8,9},{9,10},{10,1... | collective-permute-start | bytes 393224 | tf_op jit(solution)/shard_map/ppermute | solution.py:519
  41.7 11.9 %collective-permute-start = (bf16[128,512]{1,0:T(8,128)(2,1)}, bf16[128,512]{1,0:T(8,128)(2,1)}, u32[]{:S(2)}, u32[]{:S(2)}) collective-permute-start(bf16[128,512]{1,0:T(8,128)(2,1)} %gated_rows.3), channel_id=1, source_target_pairs={{0,3},{1,0},{2,1},{3,2},{4,7},{5,4},{6,5},{7,6},{8,11},{9,8},{10,9... | collective-permute-start | bytes 393224 | tf_op jit(solution)/shard_map/ppermute | solution.py:519
  46.0 1.0 copy-start.4
  52.2 1.4 %copy-start.5 = (f32[2048]{0:T(1024)S(1)}, f32[2048]{0:T(1024)}, u32[]{:S(2)}) copy-start(f32[2048]{0:T(1024)} %param.24) | copy-start | bytes 24580
  53.6 37.4 %copy-start.1 = (bf16[1,2048,1024]{2,1,0:T(8,128)(2,1)S(1)}, bf16[1,2048,1024]{2,1,0:T(8,128)(2,1)}, u32[]{:S(2)}) copy-start(bf16[1,2048,1024]{2,1,0:T(8,128)(2,1)} %up_ref.1) | copy-start | bytes 12582916
  53.6 37.4 %copy-start.2 = (bf16[1,1024,2048]{2,1,0:T(8,128)(2,1)S(1)}, bf16[1,1024,2048]{2,1,0:T(8,128)(2,1)}, u32[]{:S(2)}) copy-start(bf16[1,1024,2048]{2,1,0:T(8,128)(2,1)} %down_ref.1) | copy-start | bytes 12582916
  56.0 35.0 %copy-start = (bf16[1,2048,1024]{2,1,0:T(8,128)(2,1)S(1)}, bf16[1,2048,1024]{2,1,0:T(8,128)(2,1)}, u32[]{:S(2)}) copy-start(bf16[1,2048,1024]{2,1,0:T(8,128)(2,1)} %gate_ref.3) | copy-start | bytes 12582916
  98.6 4.0 %copy-start.7 = (f32[128,2]{0,1:T(2,128)S(1)}, f32[128,2]{0,1:T(2,128)}, u32[]{:S(2)}) copy-start(f32[128,2]{0,1:T(2,128)} %param.26) | copy-start | bytes 3076
  98.6 34.9 %copy-start.3 = (bf16[512,1024]{1,0:T(8,128)(2,1)S(1)}, bf16[512,1024]{1,0:T(8,128)(2,1)}, u32[]{:S(2)}) copy-start(bf16[512,1024]{1,0:T(8,128)(2,1)} %get-tuple-element.33.pick_ref) | copy-start | bytes 3145732
  98.6 34.8 %all-to-all-start.3 = ((bf16[128,8,1024]{2,1,0:T(8,128)(2,1)}), bf16[128,8,1024]{2,1,0:T(8,128)(2,1)S(1)}, u32[]{:S(2)}, u32[]{:S(2)}) async-start(bf16[128,8,1024]{2,1,0:T(8,128)(2,1)} %bitcast.17), calls=%async_computation.3 | async-start | bytes 4194304 | tf_op jit(solution)/shard_map/all_to_all | solution.py:527

commit v5 on v4

--- a/solution.py
+++ b/solution.py
@@ -55,7 +55,7 @@
     return high, (value - high.astype(F32)).astype(BF16)
 
 
-def state_kernel(forget_ref, value_ref, margin_ref, spike_ref, cum_ref, values_ref, start_ref, sent_ref, state, before, keys_in, decays):
+def state_kernel(forget_ref, value_ref, margin_ref, spike_ref, cum_ref, start_ref, sent_ref, state, before, keys_in, decays):
     step = pl.program_id(0)
     heads = forget_ref.shape[1] // DK
 
@@ -87,7 +87,6 @@
             last = cum[CHUNK - 1 : CHUNK, :]
             logits = value_ref[rows, cols].astype(F32)
             values = (logits * sigmoid(logits)).astype(BF16)
-            values_ref[rows, cols] = values
             kept = (keys_in[rows, cols] * jnp.exp(last - cum)).astype(BF16)
             state[cols, :] = jnp.exp(last) * state[cols, :] + dot_tn(values, kept)
             before[:, cols] = before[:, cols] + last
@@ -126,13 +125,11 @@
         ],
         out_specs=[
             pl.BlockSpec((size, width), by_rows),
-            pl.BlockSpec((size, width), by_rows),
             pl.BlockSpec((size // CHUNK, width, DK), lambda i: (i, 0, 0)),
             pl.BlockSpec((heads * 8, DK // 8 + TAIL, DK), lambda i: (0, 0, 0)),
         ],
         out_shape=[
             pltpu.HBM((rows, width), F32),
-            pltpu.HBM((rows, width), BF16),
             pltpu.HBM((rows // CHUNK, width, DK), F32),
             pltpu.HBM((heads * 8, DK // 8 + TAIL, DK), BF16),
         ],
@@ -170,7 +167,7 @@
     return dot_nt(queries[0], states[0]) + dot_nt(queries[0], states[1]) + dot_nt(queries[1], states[0])
 
 
-def within_kernel(query_ref, forget_ref, margin_ref, cum_ref, values_ref, start_ref, gate_ref, scale_ref, out_ref, high_ref, low_ref, gates_ref, before):
+def within_kernel(query_ref, forget_ref, margin_ref, cum_ref, value_ref, start_ref, gate_ref, scale_ref, out_ref, high_ref, low_ref, gates_ref, before):
     heads = query_ref.shape[1] // DK
     causal = lower_mask(CHUNK, False)
 
@@ -188,7 +185,8 @@
         scores = jnp.where(causal, scores, 0.0).astype(BF16)
         decayed = queries * jnp.exp(cum)
         earlier = dot_split(halves(decayed), halves(start_ref[0, cols, :]))
-        out_ref[:, cols] = dot_nn(scores, values_ref[:, cols]) + earlier
+        logits = value_ref[:, cols].astype(F32)
+        out_ref[:, cols] = dot_nn(scores, (logits * sigmoid(logits)).astype(BF16)) + earlier
         high_ref[:, cols], low_ref[:, cols] = halves(decayed * jnp.exp(before[:, cols]))
         before[:, cols] = before[:, cols] + cum[CHUNK - 1 : CHUNK, :]
         logits = gate_ref[:, cols].astype(F32)
@@ -504,11 +502,11 @@
     width = resid.shape[1]
     margin = forget_margin[None, :]
     places = lax.axis_size("tp")
-    cum, values, start, sent = local_states(forget_logits, value_logits, margin, decay_spike.T)
+    cum, start, sent = local_states(forget_logits, value_logits, margin, decay_spike.T)
     select, pick = slots_of(routes, experts, capacity)
     parts = lax.all_to_all(sent, SP, split_axis=0, concat_axis=0, tiled=True)
     within, high, low, gates = within_blocks(
-        query, forget_logits, margin, cum, values, start, output_gate_logits, head_norm_scale[None, :]
+        query, forget_logits, margin, cum, value_logits, start, output_gate_logits, head_norm_scale[None, :]
     )
     prior = lax.all_to_all(carried_in(parts), SP, split_axis=0, concat_axis=0, tiled=True)
     prior = prior.reshape(start.shape[1], DK)

time: 137 us -> 137 us (level)
  no operation moved by 1% of the time
where the time goes in v5:
time: 137 us; the launch traced here: 136 us
  blocking collectives  52.8 us (39%)
  waiting for transfers between devices  35 us (26%)
  Pallas kernels  33.4 us (24%)
  starting transfers between devices  13.2 us (10%)
    all_to_all x1, blocking collectives, body(): lax.all_to_all(packed.reshape(shape), SP_TP, split_axis=0, concat_axis=0,...  34.9 us
    all_to_all x1, waiting for transfers between devices, body(): lax.all_to_all(answers.reshape(shape), SP_TP, split_axis=0, concat_axis=0...  30.8 us
    all_to_all x1, blocking collectives, body(): parts = lax.all_to_all(sent, SP, split_axis=0, concat_axis=0, tiled=True)  17.8 us
    pallas_call x1, Pallas kernels, experts_on(): pl.pallas_call(expert_kernel, in_specs=[here, here, here, here], out_spec...  7.58 us
    ppermute x3, starting transfers between devices, body(): lax.ppermute(gated, 'tp', [(i, (i + k) % places) for i in range(places)])  5.42 us
    pallas_call x1, Pallas kernels, within_blocks(): pl.pallas_call(within_kernel, grid=(rows // CHUNK,), in_specs=[block, blo...  4.67 us
    all_to_all x1, waiting for transfers between devices, body(): lax.all_to_all(carried_in(parts), SP, split_axis=0, concat_axis=0, tiled=...  4.2 us
    all_to_all x1, starting transfers between devices, body(): lax.all_to_all(answers.reshape(shape), SP_TP, split_axis=0, concat_axis=0...  3.94 us
  transfers between devices with their start and end apart: 5, of which 2 were waited for; matrix products, arithmetic and copies ran while one was open for 0% of the time, Pallas kernels for 11%

profile of v5, /device:TPU:1, one launch (start us, length us, event | category | flops | bytes accessed | tf_op | source)
XLA Modules:
  0.0 136.0 jit_solution(17522532839445965796)
XLA Ops:
  0.0 3.8 %local_states.1 = (f32[512,512]{1,0:T(8,128)}, f32[4,512,128]{2,1,0:T(8,128)}, bf16[32,24,128]{2,1,0:T(8,128)(2,1)}) custom-call(bf16[512,512]{1,0:T(8,128)(2,1)} %forget_ref.3, bf16[512,512]{1,0:T(8,128)(2,1)} %value_ref.3, f32[1,512]{1,0:T(1,128)} %bitcast.18, f32[4,512]{1,0:T(4,128)} %bitcast.20), custom_call_target="tpu_custom_call" | custom-call | tf_op jit(solution)/shard_map/local_states/pallas_call | solution.py:117
  3.8 17.8 %all_to_all.20.parts_ref = bf16[32,24,128]{2,1,0:T(8,128)(2,1)S(1)} all-to-all(bf16[32,24,128]{2,1,0:T(8,128)(2,1)} %get-tuple-element.24), channel_id=1, replica_groups=mesh['sp_0'=4,'sp_1'=4,'sp_2'=2,'tp'=4] {'sp_0','sp_1','sp_2'}, dimensions={0} | all-to-all | bytes 393216 | tf_op jit(solution)/shard_map/all_to_all | solution.py:507
  21.6 0.8 carried_in.1
  22.4 3.8 %all-to-all-start.1 = ((f32[32,16,128]{2,1,0:T(8,128)}), f32[32,16,128]{2,1,0:T(8,128)S(1)}, u32[]{:S(2)}, u32[]{:S(2)}) async-start(f32[32,16,128]{2,1,0:T(8,128)} %carried_in.1), calls=%async_computation.1 | async-start | bytes 524288 | tf_op jit(solution)/shard_map/all_to_all | solution.py:511
  26.2 4.7 %within_blocks.1 = (f32[512,512]{1,0:T(8,128)S(1)}, bf16[512,512]{1,0:T(8,128)(2,1)S(1)}, bf16[512,512]{1,0:T(8,128)(2,1)S(1)}, f32[512,512]{1,0:T(8,128)S(1)}) custom-call(bf16[512,512]{1,0:T(8,128)(2,1)} %query_ref.1, bf16[512,512]{1,0:T(8,128)(2,1)} %forget_ref.3, f32[1,512]{1,0:T(1,128)} %bitcast.19, f32[512,512]{1,0:T(8,128)} %get-tuple-element.19.cum_ref, ...), custom_call_target="tpu_custom_call" | custom-call | tf_op jit(solution)/shard_map/within_blocks/pallas_call | solution.py:200
  30.9 4.2 %all-to-all-done.1 = f32[32,16,128]{2,1,0:T(8,128)S(1)} async-done(((f32[32,16,128]{2,1,0:T(8,128)}), f32[32,16,128]{2,1,0:T(8,128)S(1)}, u32[]{:S(2)}, u32[]{:S(2)}) %all-to-all-start.1) | async-done | bytes 262176 | tf_op jit(solution)/shard_map/all_to_all | solution.py:511
  35.1 1.2 gated_rows.5
  36.2 2.7 %collective-permute-start.2 = (bf16[128,512]{1,0:T(8,128)(2,1)}, bf16[128,512]{1,0:T(8,128)(2,1)}, u32[]{:S(2)}, u32[]{:S(2)}) collective-permute-start(bf16[128,512]{1,0:T(8,128)(2,1)} %gated_rows.5), channel_id=1, source_target_pairs={{0,2},{1,3},{2,0},{3,1},{4,6},{5,7},{6,4},{7,5},{8,10},{9,11},{10,... | collective-permute-start | bytes 393224 | tf_op jit(solution)/shard_map/ppermute | solution.py:517
  39.0 1.1 gated_rows.4
  40.1 0.3 collective-permute-start.1
  40.4 1.2 gated_rows.3
  41.6 2.4 %collective-permute-start = (bf16[128,512]{1,0:T(8,128)(2,1)}, bf16[128,512]{1,0:T(8,128)(2,1)}, u32[]{:S(2)}, u32[]{:S(2)}) collective-permute-start(bf16[128,512]{1,0:T(8,128)(2,1)} %gated_rows.3), channel_id=1, source_target_pairs={{0,3},{1,0},{2,1},{3,2},{4,7},{5,4},{6,5},{7,6},{8,11},{9,8},{10,9... | collective-permute-start | bytes 393224 | tf_op jit(solution)/shard_map/ppermute | solution.py:517
  44.0 0.1 copy.16.routes_ref
  44.1 1.8 %slots_of.1 = (bf16[1024,256]{1,0:T(8,128)(2,1)}, bf16[512,1024]{1,0:T(8,128)(2,1)}) custom-call(s32[128,2]{1,0:T(8,128)S(1)} %copy.16.routes_ref), custom_call_target="tpu_custom_call" | custom-call | tf_op jit(solution)/shard_map/slots_of/pallas_call | solution.py:275
  45.9 1.0 copy-done.4
  46.9 3.8 %project_own.1 = (f32[128,2048]{1,0:T(8,128)S(1)}, bf16[2048,2048]{1,0:T(8,128)(2,1)S(1)}, bf16[1024,256]{1,0:T(8,128)(2,1)S(1)}) custom-call(f32[512,512]{1,0:T(8,128)S(1)} %get-tuple-element.21.refs_0_.within_ref, bf16[512,512]{1,0:T(8,128)(2,1)S(1)} %get-tuple-element.22.refs_1_.high_ref, bf16[512,512]{1,0:T(8,128)(2,1)S(1)} %get-tuple-element.23.refs_2_.low_ref, ...), custom_call_target="tpu_custom_call" | custom-call | tf_op jit(solution)/shard_map/project_own/pallas_call | solution.py:306
  50.7 1.4 project_more.2.total_ref
  52.1 0.0 copy-start.5
  52.1 0.0 collective-permute-done.1.part_ref
  52.1 1.4 project_more.3.total_ref
  53.5 0.0 collective-permute-done.part_ref
  53.5 0.0 copy-start.1
  53.5 0.0 copy-start.2
  53.5 2.4 %project.1 = (bf16[128,2048]{1,0:T(8,128)(2,1)}, bf16[1024,1024]{1,0:T(8,128)(2,1)S(1)}) custom-call(bf16[128,512]{1,0:T(8,128)(2,1)} %collective-permute-done.part_ref, bf16[2048,2048]{1,0:T(8,128)(2,1)S(1)} %get-tuple-element.27.matrix_ref, f32[128,2048]{1,0:T(8,128)S(1)} %project_more.3.total_ref, f32[1,2048]{1,0:T(1,128)S(1)} %bitcast.16, ...), custom_call_target="tpu_custom_call" | custom-call | tf_op jit(solution)/shard_map/project/pallas_call | solution.py:367
  55.9 0.0 copy-start
  55.9 34.9 %all_to_all.21 = bf16[128,8,1024]{2,1,0:T(8,128)(2,1)S(1)} all-to-all(bf16[128,8,1024]{2,1,0:T(8,128)(2,1)S(1)} %bitcast.15), channel_id=1, replica_groups=mesh['sp_0'=4,'sp_1'=4,'sp_2'=2,'tp'=4] {'sp_0','sp_1','sp_2','tp'}, dimensions={0} | all-to-all | bytes 4194304 | tf_op jit(solution)/shard_map/all_to_all | solution.py:523
  90.9 7.6 %experts_on.1 = bf16[1024,1024]{1,0:T(8,128)(2,1)} custom-call(bf16[1024,1024]{1,0:T(8,128)(2,1)S(1)} %bitcast.10, bf16[1,2048,1024]{2,1,0:T(8,128)(2,1)S(1)} %copy-done, bf16[1,2048,1024]{2,1,0:T(8,128)(2,1)S(1)} %copy-done.1, bf16[1,1024,2048]{2,1,0:T(8,128)(2,1)S(1)} %copy-done.2), custom_call_target="tpu_custom_call" | custom-call | tf_op jit(solution)/shard_map/experts_on/pallas_call | solution.py:422
  98.5 0.0 copy-start.7
  98.5 3.9 %all-to-all-start.3 = ((bf16[128,8,1024]{2,1,0:T(8,128)(2,1)}), bf16[128,8,1024]{2,1,0:T(8,128)(2,1)S(1)}, u32[]{:S(2)}, u32[]{:S(2)}) async-start(bf16[128,8,1024]{2,1,0:T(8,128)(2,1)} %bitcast.17), calls=%async_computation.3 | async-start | bytes 4194304 | tf_op jit(solution)/shard_map/all_to_all | solution.py:525
  102.4 0.1 copy.17.weight_ref
  102.6 30.8 %all-to-all-done.3 = bf16[128,8,1024]{2,1,0:T(8,128)(2,1)S(1)} async-done(((bf16[128,8,1024]{2,1,0:T(8,128)(2,1)}), bf16[128,8,1024]{2,1,0:T(8,128)(2,1)S(1)}, u32[]{:S(2)}, u32[]{:S(2)}) %all-to-all-start.3) | async-done | bytes 2097184 | tf_op jit(solution)/shard_map/all_to_all | solution.py:525
  133.3 2.5 %combine.1 = bf16[128,2048]{1,0:T(8,128)(2,1)} custom-call(bf16[1024,1024]{1,0:T(8,128)(2,1)S(1)} %bitcast.9, bf16[512,1024]{1,0:T(8,128)(2,1)S(1)} %copy-done.3, f32[128,2]{1,0:T(8,128)S(1)} %copy.17.weight_ref, bf16[128,2048]{1,0:T(8,128)(2,1)} %get-tuple-element.32.stream_ref), custom_call_target="tpu_custom_call" | custom-call | tf_op jit(solution)/shard_map/combine/pallas_call | solution.py:467
  (11 shorter events, 0.0 us)
Async XLA Ops:
  22.4 12.7 %all-to-all-start.1 = ((f32[32,16,128]{2,1,0:T(8,128)}), f32[32,16,128]{2,1,0:T(8,128)S(1)}, u32[]{:S(2)}, u32[]{:S(2)}) async-start(f32[32,16,128]{2,1,0:T(8,128)} %carried_in.1), calls=%async_computation.1 | async-start | bytes 524288 | tf_op jit(solution)/shard_map/all_to_all | solution.py:511
  36.2 7.7 %copy-start.6 = (s32[128,2]{0,1:T(2,128)S(1)}, s32[128,2]{0,1:T(2,128)}, u32[]{:S(2)}) copy-start(s32[128,2]{0,1:T(2,128)} %param.25) | copy-start | bytes 3076
  36.2 14.5 %collective-permute-start.2 = (bf16[128,512]{1,0:T(8,128)(2,1)}, bf16[128,512]{1,0:T(8,128)(2,1)}, u32[]{:S(2)}, u32[]{:S(2)}) collective-permute-start(bf16[128,512]{1,0:T(8,128)(2,1)} %gated_rows.5), channel_id=1, source_target_pairs={{0,2},{1,3},{2,0},{3,1},{4,6},{5,7},{6,4},{7,5},{8,10},{9,11},{10,... | collective-permute-start | bytes 393224 | tf_op jit(solution)/shard_map/ppermute | solution.py:517
  40.1 12.0 %collective-permute-start.1 = (bf16[128,512]{1,0:T(8,128)(2,1)}, bf16[128,512]{1,0:T(8,128)(2,1)}, u32[]{:S(2)}, u32[]{:S(2)}) collective-permute-start(bf16[128,512]{1,0:T(8,128)(2,1)} %gated_rows.4), channel_id=1, source_target_pairs={{0,1},{1,2},{2,3},{3,0},{4,5},{5,6},{6,7},{7,4},{8,9},{9,10},{10,1... | collective-permute-start | bytes 393224 | tf_op jit(solution)/shard_map/ppermute | solution.py:517
  41.6 11.9 %collective-permute-start = (bf16[128,512]{1,0:T(8,128)(2,1)}, bf16[128,512]{1,0:T(8,128)(2,1)}, u32[]{:S(2)}, u32[]{:S(2)}) collective-permute-start(bf16[128,512]{1,0:T(8,128)(2,1)} %gated_rows.3), channel_id=1, source_target_pairs={{0,3},{1,0},{2,1},{3,2},{4,7},{5,4},{6,5},{7,6},{8,11},{9,8},{10,9... | collective-permute-start | bytes 393224 | tf_op jit(solution)/shard_map/ppermute | solution.py:517
  45.9 1.0 copy-start.4
  52.1 1.4 %copy-start.5 = (f32[2048]{0:T(1024)S(1)}, f32[2048]{0:T(1024)}, u32[]{:S(2)}) copy-start(f32[2048]{0:T(1024)} %param.24) | copy-start | bytes 24580
  53.5 37.4 %copy-start.1 = (bf16[1,2048,1024]{2,1,0:T(8,128)(2,1)S(1)}, bf16[1,2048,1024]{2,1,0:T(8,128)(2,1)}, u32[]{:S(2)}) copy-start(bf16[1,2048,1024]{2,1,0:T(8,128)(2,1)} %up_ref.1) | copy-start | bytes 12582916
  53.5 37.4 %copy-start.2 = (bf16[1,1024,2048]{2,1,0:T(8,128)(2,1)S(1)}, bf16[1,1024,2048]{2,1,0:T(8,128)(2,1)}, u32[]{:S(2)}) copy-start(bf16[1,1024,2048]{2,1,0:T(8,128)(2,1)} %down_ref.1) | copy-start | bytes 12582916
  55.9 35.0 %copy-start = (bf16[1,2048,1024]{2,1,0:T(8,128)(2,1)S(1)}, bf16[1,2048,1024]{2,1,0:T(8,128)(2,1)}, u32[]{:S(2)}) copy-start(bf16[1,2048,1024]{2,1,0:T(8,128)(2,1)} %gate_ref.3) | copy-start | bytes 12582916
  98.5 4.0 %copy-start.7 = (f32[128,2]{0,1:T(2,128)S(1)}, f32[128,2]{0,1:T(2,128)}, u32[]{:S(2)}) copy-start(f32[128,2]{0,1:T(2,128)} %param.26) | copy-start | bytes 3076
  98.5 34.9 %copy-start.3 = (bf16[512,1024]{1,0:T(8,128)(2,1)S(1)}, bf16[512,1024]{1,0:T(8,128)(2,1)}, u32[]{:S(2)}) copy-start(bf16[512,1024]{1,0:T(8,128)(2,1)} %get-tuple-element.31.pick_ref) | copy-start | bytes 3145732
  98.5 34.8 %all-to-all-start.3 = ((bf16[128,8,1024]{2,1,0:T(8,128)(2,1)}), bf16[128,8,1024]{2,1,0:T(8,128)(2,1)S(1)}, u32[]{:S(2)}, u32[]{:S(2)}) async-start(bf16[128,8,1024]{2,1,0:T(8,128)(2,1)} %bitcast.17), calls=%async_computation.3 | async-start | bytes 4194304 | tf_op jit(solution)/shard_map/all_to_all | solution.py:525
